TPU v7x, 32 devices: a whole 2x2x4 slice. The times are simulated.
32 devices in a mesh: sp: 4 (over y, x), tp: 8 (over z, core).
Axes of the slice: x: 2, y: 2, z: 4, core: 2. Of those that a mesh axis runs over, the one named last changes fastest.
Arguments:
- resid: bfloat16 [2048, 2048], P(('sp', 'tp')), may hold values from -6 to 6
- query_a: bfloat16 [2048, 16, 128], P('sp', 'tp'), may hold values from -16 to 16
- key_a: bfloat16 [2048, 16, 128], P('sp', 'tp'), may hold values from -16 to 16
- value_a: bfloat16 [2048, 16, 128], P('sp', 'tp'), may hold values from -6 to 6
- query_b: bfloat16 [2048, 16, 64], P('sp', 'tp'), may hold values from -16 to 16
- key_b: bfloat16 [2048, 16, 64], P('sp', 'tp'), may hold values from -16 to 16
- value_b: bfloat16 [2048, 16, 64], P('sp', 'tp'), may hold values from -6 to 6
- mix_a: float32 [16], P('tp'), may hold values from 0.3 to 0.8
- mix_b: float32 [16], P('tp'), may hold values from 0.3 to 0.8
- head_gain_a: float32 [128], replicated, may hold values from 0.1 to 1.9
- head_gain_b: float32 [64], replicated, may hold values from 0.1 to 1.9
- proj_a: bfloat16 [2048, 2048], P('tp'), may hold values from -0.109375 to 0.109375
- proj_b: bfloat16 [1024, 2048], P('tp'), may hold values from -0.109375 to 0.109375
- norm_gain: float32 [2048], replicated, may hold values from 0.1 to 1.9
- route_ids: int32 [2048, 2], P(('sp', 'tp')), may hold values from 0 to 3, all different within a row; in each aligned block of 64 rows (0 to 63, 64 to 127, ...) at most 48 rows name the same one
- route_weights: float32 [2048, 2], P(('sp', 'tp')), may hold values from 0.2 to 1
- expert_gate: bfloat16 [4, 2048, 6144], P('sp', None, 'tp'), may hold values from -0.125 to 0.125
- expert_up: bfloat16 [4, 2048, 6144], P('sp', None, 'tp'), may hold values from -0.125 to 0.125
- expert_down: bfloat16 [4, 6144, 2048], P('sp', 'tp'), may hold values from -0.078125 to 0.078125
Outputs:
- out: bfloat16 [2048, 2048], P(('sp', 'tp'))
Inputs may be any that keep to these rules, and one draw needn't show every extreme that they name: `route_ids`: each row names 2 different experts. Within the rows of one device (aligned blocks of 64 rows) no expert is named by more than 48 rows, and in every draw some device's block names some expert exactly 48 times.
All inputs are finite; a program needn't handle non-finite values.
Results may differ from a plain program's by a relative error of at most 0.02.
Values may be sent and summed in bfloat16 or wider, within the bound.
A program may use at most 128 MiB of HBM per device.

v0:
```python
import functools
import math

import jax
import jax.numpy as jnp
import numpy as np
from jax import lax
from jax.experimental import pallas as pl
from jax.experimental.pallas import tpu as pltpu
from jax.sharding import PartitionSpec as P

EPS = 1e-06
NEG = -1e30
HEAD_SCALE = 1.0 - (0.8 - 0.6 * math.exp(-0.3))
KEY_STEP = 512


def partner(value, axis, apart):
    return lax.ppermute(value, axis, [(i, i ^ 1 << apart) for i in range(lax.axis_size(axis))])


def rms_scaled(values, gain):
    return values * lax.rsqrt(jnp.mean(values * values, axis=-1, keepdims=True) + EPS) * gain


def slot_numbers(route_rows, experts, capacity):
    count, top_count = route_rows.shape
    flat = route_rows.reshape(count * top_count)
    onehot = (flat[:, None] == jnp.arange(experts, dtype=jnp.int32)[None, :]).astype(jnp.int32)
    ranks = jnp.sum((jnp.cumsum(onehot, axis=0) - onehot) * onehot, axis=1)
    return (flat * capacity + ranks).reshape(count, top_count)


def empty_map(count, heads, width):
    return (
        jnp.zeros((count, heads, width), jnp.float32),
        jnp.full((heads, count), NEG, jnp.float32),
        jnp.zeros((heads, count), jnp.float32),
    )


def empty_group(query, value):
    return (
        empty_map(query.shape[0], query.shape[1], value.shape[2]),
        empty_map(query.shape[0], query.shape[1], value.shape[2]),
    )


def map_update(state, query, keys, values, allowed, scale):
    weighted, maximum, sums = state
    scores = jnp.einsum("qhd,khd->hqk", query, keys, preferred_element_type=jnp.float32) * scale
    scores = jnp.where(allowed[None], scores, NEG)
    fresh = jnp.maximum(maximum, jnp.max(scores, axis=2))
    weights = jnp.where(allowed[None], jnp.exp(scores - fresh[:, :, None]), 0.0)
    factor = jnp.exp(maximum - fresh)
    sums = sums * factor + jnp.sum(weights, axis=2)
    added = jnp.einsum(
        "hqk,khv->qhv", weights.astype(jnp.bfloat16), values, preferred_element_type=jnp.float32
    )
    weighted = weighted * jnp.transpose(factor)[:, :, None] + added
    return (weighted, fresh, sums)


def group_update(states, query, keys, values, allowed):
    width = query.shape[2] // 2
    scale = 1.0 / math.sqrt(width)
    return tuple(
        (
            map_update(
                states[which],
                query[:, :, which * width : (which + 1) * width],
                keys[:, :, which * width : (which + 1) * width],
                values,
                allowed,
                scale,
            )
            for which in range(2)
        )
    )


def set_update(carry, queries, pieces):
    rows_a, rows_b, query_pos = queries
    piece_key_a, piece_value_a, piece_key_b, piece_value_b = pieces
    length = piece_key_a.shape[0]
    step = math.gcd(length, KEY_STEP)
    latest = query_pos[-1]

    def inner(index, states):
        first = index * step

        def compute(current):
            keys_a = lax.dynamic_slice_in_dim(piece_key_a, first, step, 0)
            values_a = lax.dynamic_slice_in_dim(piece_value_a, first, step, 0)
            keys_b = lax.dynamic_slice_in_dim(piece_key_b, first, step, 0)
            values_b = lax.dynamic_slice_in_dim(piece_value_b, first, step, 0)
            key_pos = first + jnp.arange(step, dtype=jnp.int32)
            allowed = key_pos[None, :] <= query_pos[:, None]
            return (
                group_update(current[0], rows_a, keys_a, values_a, allowed),
                group_update(current[1], rows_b, keys_b, values_b, allowed),
            )

        return lax.cond(first <= latest, compute, lambda current: current, states)

    return lax.fori_loop(0, length // step, inner, carry)


def finish_group(states, mix, gain):
    outputs = [state[0] / jnp.transpose(state[2])[:, :, None] for state in states]
    mixed = outputs[0] - mix[None, :, None] * outputs[1]
    normed = rms_scaled(mixed, gain) * HEAD_SCALE
    return normed.astype(jnp.bfloat16).reshape(mixed.shape[0], -1)


def greet(axis, ways):
    me = lax.axis_index(axis)
    barrier = pltpu.get_barrier_semaphore()
    for apart in range(1, ways):
        pl.semaphore_signal(
            barrier,
            inc=1,
            device_id={axis: lax.rem(me + apart, ways)},
            device_id_type=pl.DeviceIdType.MESH,
        )
    pl.semaphore_wait(barrier, ways - 1)


def heads_kernel(
    units,
    chunk,
    qa_ref,
    ka_ref,
    va_ref,
    qb_ref,
    kb_ref,
    vb_ref,
    par_ref,
    out_ref,
    got_q,
    got_k,
    got_v,
    heads,
    send_in,
    recv_in,
    send_out,
    recv_out,
):
    me = lax.axis_index("sp")
    ways, rows, wide = got_q.shape
    greet("sp", ways)
    refs = {"a": (qa_ref, ka_ref, va_ref), "b": (qb_ref, kb_ref, vb_ref)}

    def unit_source(unit, kind):
        group, head = units[unit]
        ref = refs[group][kind]
        return ref.at[:, head * wide : (head + 1) * wide] if group == "a" else ref

    def unit_copy(unit, kind, landing, slot):
        return pltpu.make_async_remote_copy(
            src_ref=unit_source(unit, kind),
            dst_ref=(got_q, got_k, got_v)[kind].at[landing],
            send_sem=send_in.at[kind, unit],
            recv_sem=recv_in.at[kind, slot],
            device_id={"sp": unit},
            device_id_type=pl.DeviceIdType.MESH,
        )

    for unit in range(ways):

        @pl.when(me != unit)
        def _():
            for kind in range(3):
                unit_copy(unit, kind, me, me).start()

        @pl.when(me == unit)
        def _():
            for kind in range(3):
                (got_q, got_k, got_v)[kind][unit] = unit_source(unit, kind)[...]

    for unit in range(ways):

        @pl.when(me != unit)
        def _():
            for kind in range(3):
                unit_copy(unit, kind, unit, unit).wait()

    par = par_ref[me]
    gain, mix = par[0:1, :], par[1:2, :]
    scale, share = par[2:3, 0:1], par[3:4, 0:1]
    valid = par[6:7, :]

    def result_copy(block):
        return pltpu.make_async_remote_copy(
            src_ref=heads.at[block],
            dst_ref=out_ref.at[me],
            send_sem=send_out.at[block],
            recv_sem=recv_out.at[me],
            device_id={"sp": block},
            device_id_type=pl.DeviceIdType.MESH,
        )

    for block in reversed(range(ways)):
        length = (block + 1) * rows

        @pl.loop(0, rows // chunk)
        def _(step):
            first = pl.multiple_of(step * chunk, chunk)
            query = got_q[block, pl.ds(first, chunk), :]
            keys = got_k[0 : block + 1].reshape(length, wide)
            values = got_v[0 : block + 1].reshape(length, wide)
            row = first + block * rows + lax.broadcasted_iota(jnp.int32, (chunk, rows), 0)
            col = block * rows + lax.broadcasted_iota(jnp.int32, (chunk, rows), 1)
            parts = []
            for which in range(2):
                picked = query * par[4 + which : 5 + which, :].astype(jnp.bfloat16)
                scores = lax.dot_general(
                    picked, keys, (((1,), (1,)), ((), ())), preferred_element_type=jnp.float32
                )
                last = jnp.where(col <= row, scores[:, block * rows :], NEG)
                if block:
                    scores = jnp.concatenate([scores[:, : block * rows], last], axis=1)
                else:
                    scores = last
                top = jnp.max(scores, axis=1, keepdims=True)
                weights = jnp.exp2((scores - top) * scale)
                sums = jnp.sum(weights, axis=1, keepdims=True)
                mixed = jnp.dot(
                    weights.astype(jnp.bfloat16), values, preferred_element_type=jnp.float32
                )
                parts.append(mixed / sums)
            mixed = parts[0] - mix * parts[1]
            square = jnp.sum(mixed * mixed * valid, axis=1, keepdims=True) * share
            heads[block, pl.ds(first, chunk), :] = (
                mixed * lax.rsqrt(square + EPS) * gain * HEAD_SCALE
            ).astype(jnp.bfloat16)

        @pl.when(me != block)
        def _():
            result_copy(block).start()

        @pl.when(me == block)
        def _():
            out_ref[block] = heads[block]

    for block in range(ways):

        @pl.when(me != block)
        def _():
            result_copy(block).wait_send()
            pltpu.make_async_remote_copy(
                src_ref=heads.at[block],
                dst_ref=out_ref.at[block],
                send_sem=send_out.at[block],
                recv_sem=recv_out.at[block],
                device_id={"sp": block},
                device_id_type=pl.DeviceIdType.MESH,
            ).wait_recv()


def whole_heads(query_a, key_a, value_a, query_b, key_b, value_b, mix_a, mix_b, gain_a, gain_b):
    ways = lax.axis_size("sp")
    heads_a, heads_b = query_a.shape[1], query_b.shape[1]
    rows, wide = query_a.shape[0], value_a.shape[2]
    order = [("a", h) for h in range(heads_a)]
    spot = heads_a // 2
    order = order[:spot] + [("b", h) for h in range(heads_b)] + order[spot:]
    fixed = np.zeros((ways, 8, wide), np.float32)
    for unit, (group, head) in enumerate(order):
        value_wide = value_a.shape[2] if group == "a" else value_b.shape[2]
        narrow = (query_a.shape[2] if group == "a" else query_b.shape[2]) // 2
        first = 0 if group == "a" else head * 2 * narrow
        fixed[unit, 2] = math.log2(math.e) / math.sqrt(narrow)
        fixed[unit, 3] = 1.0 / value_wide
        fixed[unit, 4, first : first + narrow] = 1.0
        fixed[unit, 5, first + narrow : first + 2 * narrow] = 1.0
        first = 0 if group == "a" else head * value_wide
        fixed[unit, 6, first : first + value_wide] = 1.0
    gains = jnp.stack(
        [gain_a if group == "a" else jnp.tile(gain_b, heads_b) for group, _ in order]
    )
    mixes = jnp.stack([(mix_a if group == "a" else mix_b)[head] for group, head in order])
    par = jnp.concatenate(
        [
            (gains * fixed[:, 6])[:, None, :],
            jnp.broadcast_to(mixes[:, None, None], (ways, 1, wide)),
            fixed[:, 2:],
        ],
        axis=1,
    )
    chunk = math.gcd(rows, 128)
    held = pltpu.VMEM((ways, rows, wide), jnp.bfloat16)
    got = pl.pallas_call(
        functools.partial(heads_kernel, order, chunk),
        out_shape=jax.ShapeDtypeStruct((ways, rows, wide), jnp.bfloat16),
        in_specs=[pl.BlockSpec(memory_space=pltpu.VMEM)] * 7,
        out_specs=pl.BlockSpec(memory_space=pltpu.VMEM),
        scratch_shapes=[
            held,
            held,
            held,
            held,
            pltpu.SemaphoreType.DMA((3, ways)),
            pltpu.SemaphoreType.DMA((3, ways)),
            pltpu.SemaphoreType.DMA((ways,)),
            pltpu.SemaphoreType.DMA((ways,)),
        ],
        compiler_params=pltpu.CompilerParams(
            collective_id=1, has_side_effects=True, vmem_limit_bytes=48 << 20
        ),
    )(
        query_a.reshape(rows, -1),
        key_a.reshape(rows, -1),
        value_a.reshape(rows, -1),
        query_b.reshape(rows, -1),
        key_b.reshape(rows, -1),
        value_b.reshape(rows, -1),
        par,
    )
    out_a = [got[at] for at, unit in enumerate(order) if unit[0] == "a"]
    out_b = [got[at] for at, unit in enumerate(order) if unit[0] == "b"]
    return jnp.concatenate(out_a, axis=1), functools.reduce(jnp.add, out_b)


def zigzag_heads(query_a, key_a, value_a, query_b, key_b, value_b, mix_a, mix_b, gain_a, gain_b):
    head_gain_a, head_gain_b = gain_a, gain_b
    seq_rows = query_a.shape[0]
    sp_ways = lax.axis_size("sp")
    place = lax.axis_index("sp")
    positions = place * seq_rows + jnp.arange(seq_rows, dtype=jnp.int32)
    levels = sp_ways.bit_length() - 1
    half = seq_rows // 2
    moved = jnp.concatenate(
        [query_a[half:].reshape(half, -1), query_b[half:].reshape(half, -1)], axis=1
    )
    for bit in range(levels):
        moved = partner(moved, "sp", bit)
    split_at = query_a.shape[1] * query_a.shape[2]
    far_a = moved[:, :split_at].reshape(half, query_a.shape[1], query_a.shape[2])
    far_b = moved[:, split_at:].reshape(half, query_b.shape[1], query_b.shape[2])
    far_pos = (sp_ways - 1 - place) * seq_rows + half + jnp.arange(half, dtype=jnp.int32)
    query_sets = ((query_a[:half], query_b[:half], positions[:half]), (far_a, far_b, far_pos))

    def fold_keys(carry, pieces):
        return tuple(
            (set_update(states, queries, pieces) for states, queries in zip(carry, query_sets))
        )

    initial = tuple(
        (
            (empty_group(queries[0], value_a), empty_group(queries[1], value_b))
            for queries in query_sets
        )
    )
    results = fold_keys(
        initial,
        (
            lax.all_gather(key_a, "sp", axis=0, tiled=True),
            lax.all_gather(value_a, "sp", axis=0, tiled=True),
            lax.all_gather(key_b, "sp", axis=0, tiled=True),
            lax.all_gather(value_b, "sp", axis=0, tiled=True),
        ),
    )
    finished = [
        (finish_group(states[0], mix_a, head_gain_a), finish_group(states[1], mix_b, head_gain_b))
        for states in results
    ]
    returned = jnp.concatenate([finished[1][0], finished[1][1]], axis=1)
    for bit in range(levels):
        returned = partner(returned, "sp", bit)
    width_a = finished[0][0].shape[1]
    heads_out_a = jnp.concatenate([finished[0][0], returned[:, :width_a]], axis=0)
    heads_out_b = jnp.concatenate([finished[0][1], returned[:, width_a:]], axis=0)
    return heads_out_a, heads_out_b


def remote(src, dst, send_sem, recv_sem, **where):
    return pltpu.make_async_remote_copy(
        src_ref=src,
        dst_ref=dst,
        send_sem=send_sem,
        recv_sem=recv_sem,
        device_id=where,
        device_id_type=pl.DeviceIdType.MESH,
    )


def greet_routes(places, chips):
    place, turn = lax.axis_index("sp"), lax.axis_index("tp")
    chip, core = lax.div(turn, 2), lax.rem(turn, 2)
    barrier = pltpu.get_barrier_semaphore()
    peers = [{"tp": 2 * chip + 1 - core}]
    peers += [{"tp": 2 * lax.rem(chip + apart, chips) + core} for apart in range(1, chips)]
    peers += [{"sp": lax.rem(place + apart, places)} for apart in range(1, places)]
    for peer in peers:
        pl.semaphore_signal(
            barrier, inc=1, device_id=peer, device_id_type=pl.DeviceIdType.MESH
        )
    pl.semaphore_wait(barrier, len(peers))


def dispatch_kernel(
    places,
    chips,
    cap,
    term_ref,
    resid_ref,
    gain_ref,
    meta_ref,
    out_ref,
    mixed_ref,
    normed_ref,
    twin,
    chip_sum,
    sums,
    near,
    stage,
    ts,
    tr,
    rs,
    rr,
    zs,
    zr,
    xs,
    xr,
    ps,
    pr,
):
    place, turn = lax.axis_index("sp"), lax.axis_index("tp")
    chip, core = lax.div(turn, 2), lax.rem(turn, 2)
    other = 2 * chip + 1 - core
    rows = normed_ref.shape[0]
    greet_routes(places, chips)

    def twin_copy(apart):
        spot = term_ref.at[lax.rem(chip + apart, chips), 1 - core]
        return remote(spot, twin.at[apart], ts.at[apart], tr.at[apart], tp=other)

    def sum_copy(apart):
        peer = 2 * lax.rem(chip + apart, chips) + core
        return remote(chip_sum.at[apart], sums.at[apart], rs.at[apart], rr.at[apart], tp=peer)

    turns = list(range(1, chips)) + [0]
    for apart in turns:
        twin_copy(apart).start()
    total = resid_ref[...].astype(jnp.float32)
    for apart in turns:
        twin_copy(apart).wait_recv()
        both = term_ref[lax.rem(chip + apart, chips), core].astype(jnp.float32) + twin[
            apart
        ].astype(jnp.float32)
        if apart:
            chip_sum[apart] = both.astype(jnp.bfloat16)
            sum_copy(apart).start()
        else:
            total = total + both
    for apart in range(1, chips):
        sum_copy(apart).wait_recv()
        total = total + sums[apart].astype(jnp.float32)
    mixed_ref[...] = total
    normed_ref[...] = rms_scaled(total, gain_ref[...]).astype(jnp.bfloat16)

    def near_copy(apart):
        peer = 2 * lax.rem(chip + apart, chips) + core
        return remote(normed_ref, near.at[apart], zs.at[apart], zr.at[apart], tp=peer)

    for apart in range(1, chips):
        near_copy(apart).start()

    def source(apart):
        return lax.rem(chip + chips - apart, chips)

    def route_copy(apart, away):
        expert = lax.rem(place + away, places)
        return remote(
            stage.at[apart, expert],
            out_ref.at[core, source(apart), place],
            xs.at[apart, away],
            xr.at[apart, away],
            sp=expert,
        )

    def pair_copy(apart, away):
        spot = out_ref.at[core, source(apart), lax.rem(place + places - away, places)]
        return remote(spot, spot, ps.at[apart, away], pr.at[apart, away], tp=other)

    slot = lax.broadcasted_iota(jnp.int32, (places * cap, rows), 0).astype(jnp.float32)
    for apart in range(chips):
        owner = 2 * source(apart) + core
        spread = jnp.zeros((places * cap, rows), jnp.float32)
        for which in range(2):
            own = meta_ref[owner, which : which + 1, 0:rows]
            spread = spread + jnp.where(slot == own, 1.0, 0.0)
        if apart:
            near_copy(apart).wait_recv()
            piece = near[apart]
        else:
            piece = normed_ref[...]
        sent = jnp.dot(spread.astype(jnp.bfloat16), piece, preferred_element_type=jnp.float32)
        stage[apart] = sent.astype(jnp.bfloat16).reshape(places, cap, sent.shape[1])
        for away in range(1, places):
            route_copy(apart, away).start()
        out_ref[core, source(apart), place] = stage[apart, place]
        pair_copy(apart, 0).start()
    for apart in range(chips):
        for away in range(1, places):
            route_copy(apart, away).wait_recv()
            pair_copy(apart, away).start()
    for apart in range(chips):
        twin_copy(apart).wait_send()
        if apart:
            sum_copy(apart).wait_send()
            near_copy(apart).wait_send()
        for away in range(places):
            if away:
                route_copy(apart, away).wait_send()
            pair_copy(apart, away).wait()


def combine_kernel(
    places,
    chips,
    cap,
    term_ref,
    meta_ref,
    mixed_ref,
    out_ref,
    pair,
    stage,
    back,
    leave,
    near,
    ps,
    pr,
    xs,
    xr,
    zs,
    zr,
):
    place, turn = lax.axis_index("sp"), lax.axis_index("tp")
    chip, core = lax.div(turn, 2), lax.rem(turn, 2)
    other = 2 * chip + 1 - core
    rows = mixed_ref.shape[0]
    greet_routes(places, chips)
    order = list(range(1, chips)) + [0]

    def source(apart):
        return lax.rem(chip + chips - apart, chips)

    def pair_copy(apart):
        return remote(
            term_ref.at[1 - core, source(apart)],
            pair.at[apart],
            ps.at[apart],
            pr.at[apart],
            tp=other,
        )

    def back_copy(apart, away):
        peer = lax.rem(place + away, places)
        return remote(
            stage.at[apart, peer],
            back.at[apart, place],
            xs.at[apart, away],
            xr.at[apart, away],
            sp=peer,
        )

    def near_copy(apart):
        peer = 2 * source(apart) + core
        return remote(leave.at[apart], near.at[apart], zs.at[apart], zr.at[apart], tp=peer)

    for apart in order:
        pair_copy(apart).start()
    for apart in order:
        pair_copy(apart).wait_recv()
        for expert in range(places):
            stage[apart, expert] = (
                term_ref[core, source(apart), expert].astype(jnp.float32)
                + pair[apart, expert].astype(jnp.float32)
            ).astype(jnp.bfloat16)
        for away in range(1, places):
            back_copy(apart, away).start()
        back[apart, place] = stage[apart, place]
    slot = lax.broadcasted_iota(jnp.int32, (places * cap, rows), 0).astype(jnp.float32)
    total = mixed_ref[...]
    for apart in order:
        owner = 2 * source(apart) + core
        gather = jnp.zeros((places * cap, rows), jnp.float32)
        for which in range(2):
            own = meta_ref[owner, which : which + 1, 0:rows]
            weight = meta_ref[owner, which + 2 : which + 3, 0:rows]
            gather = gather + jnp.where(slot == own, weight, 0.0)
        high = gather.astype(jnp.bfloat16)
        low = (gather - high.astype(jnp.float32)).astype(jnp.bfloat16)
        for away in range(1, places):
            back_copy(apart, away).wait_recv()
        held = back[apart].reshape(places * cap, back.shape[3])
        dims = (((0,), (0,)), ((), ()))
        part = lax.dot_general(high, held, dims, preferred_element_type=jnp.float32)
        part = part + lax.dot_general(low, held, dims, preferred_element_type=jnp.float32)
        if apart:
            leave[apart] = part.astype(jnp.bfloat16)
            near_copy(apart).start()
        else:
            total = total + part
    for apart in range(1, chips):
        near_copy(apart).wait_recv()
        total = total + near[apart].astype(jnp.float32)
    out_ref[...] = total.astype(jnp.bfloat16)
    for apart in range(chips):
        if apart:
            near_copy(apart).wait_send()
        pair_copy(apart).wait_send()
        for away in range(1, places):
            back_copy(apart, away).wait_send()


def vmem(count):
    return [pl.BlockSpec(memory_space=pltpu.VMEM)] * count


def routed_experts(term, resid, norm_gain, meta, capacity, expert_gate, expert_up, expert_down):
    places, chips = lax.axis_size("sp"), lax.axis_size("tp") // 2
    rows, width = resid.shape
    shape = (2, chips, places, capacity, width)
    sems = pltpu.SemaphoreType.DMA
    half = pltpu.VMEM((chips, places, capacity, width), jnp.bfloat16)
    piece_rows = pltpu.VMEM((chips, rows, width), jnp.bfloat16)
    piece, mixed = pl.pallas_call(
        functools.partial(dispatch_kernel, places, chips, capacity),
        out_shape=(
            jax.ShapeDtypeStruct(shape, jnp.bfloat16),
            jax.ShapeDtypeStruct((rows, width), jnp.float32),
        ),
        in_specs=vmem(4),
        out_specs=vmem(2),
        scratch_shapes=[
            pltpu.VMEM((rows, width), jnp.bfloat16),
            piece_rows,
            piece_rows,
            piece_rows,
            piece_rows,
            half,
            sems((chips,)),
            sems((chips,)),
            sems((chips,)),
            sems((chips,)),
            sems((chips,)),
            sems((chips,)),
            sems((chips, places)),
            sems((chips, places)),
            sems((chips, places)),
            sems((chips, places)),
        ],
        compiler_params=pltpu.CompilerParams(
            collective_id=2, has_side_effects=True, vmem_limit_bytes=48 << 20
        ),
    )(term.reshape(chips, 2, rows, width), resid, norm_gain[None, :], meta)
    piece = piece.reshape(-1, width)
    gate = jnp.dot(piece, expert_gate[0], preferred_element_type=jnp.float32)
    upward = jnp.dot(piece, expert_up[0], preferred_element_type=jnp.float32)
    hidden = (jax.nn.silu(gate) * upward).astype(jnp.bfloat16)
    term = jnp.dot(hidden, expert_down[0], preferred_element_type=jnp.float32)
    return pl.pallas_call(
        functools.partial(combine_kernel, places, chips, capacity),
        out_shape=jax.ShapeDtypeStruct((rows, width), jnp.bfloat16),
        in_specs=vmem(3),
        out_specs=vmem(1)[0],
        scratch_shapes=[
            half,
            half,
            half,
            piece_rows,
            piece_rows,
            sems((chips,)),
            sems((chips,)),
            sems((chips, places)),
            sems((chips, places)),
            sems((chips,)),
            sems((chips,)),
        ],
        compiler_params=pltpu.CompilerParams(
            collective_id=3, has_side_effects=True, vmem_limit_bytes=56 << 20
        ),
    )(term.astype(jnp.bfloat16).reshape(shape), meta, mixed)


def per_device(
    resid,
    query_a,
    key_a,
    value_a,
    query_b,
    key_b,
    value_b,
    mix_a,
    mix_b,
    head_gain_a,
    head_gain_b,
    proj_a,
    proj_b,
    norm_gain,
    route_ids,
    route_weights,
    expert_gate,
    expert_up,
    expert_down,
):
    sp_ways = lax.axis_size("sp")
    fits = query_a.shape[1] + query_b.shape[1] == sp_ways
    whole_b = query_b.shape[1] * query_b.shape[2] == query_a.shape[2]
    whole_b = whole_b and query_b.shape[2] == value_b.shape[2]
    fits = fits and query_a.shape[2] == value_a.shape[2] and whole_b
    attend = whole_heads if fits else zigzag_heads
    heads_out_a, heads_out_b = attend(
        query_a,
        key_a,
        value_a,
        query_b,
        key_b,
        value_b,
        mix_a,
        mix_b,
        head_gain_a,
        head_gain_b,
    )
    width = resid.shape[1]
    tok_rows = resid.shape[0]
    top_count = route_ids.shape[1]
    capacity = 3 * top_count * tok_rows // (2 * sp_ways)
    own_slots = slot_numbers(route_ids, sp_ways, capacity)
    term = jnp.dot(heads_out_a, proj_a, preferred_element_type=jnp.float32)
    term = term + jnp.dot(heads_out_b, proj_b, preferred_element_type=jnp.float32)
    tp_ways = lax.axis_size("tp")
    if top_count == 2 and capacity % 16 == 0 and tok_rows <= 128 and tp_ways % 2 == 0:
        meta = jnp.concatenate([own_slots.astype(jnp.float32).T, route_weights.T], axis=0)
        meta = jnp.pad(meta, ((0, 4), (0, 128 - tok_rows)))
        meta = lax.all_gather(meta, "tp", axis=0)
        return routed_experts(
            term.astype(jnp.bfloat16),
            resid,
            norm_gain,
            meta,
            capacity,
            expert_gate,
            expert_up,
            expert_down,
        )
    mixed = resid.astype(jnp.float32) + lax.psum_scatter(
        lax.optimization_barrier(term.astype(jnp.bfloat16))
        .astype(jnp.float32)
        .astype(jnp.bfloat16),
        "tp",
        scatter_dimension=0,
        tiled=True,
    ).astype(jnp.float32)
    normed = rms_scaled(mixed, norm_gain).astype(jnp.bfloat16)
    lookup = jnp.arange(sp_ways * capacity, dtype=jnp.int32)[:, None]
    spread = jnp.zeros((sp_ways * capacity, tok_rows), jnp.float32)
    for which in range(top_count):
        spread = spread + (own_slots[:, which][None, :] == lookup).astype(jnp.float32)
    outgoing = jnp.dot(
        spread.astype(jnp.bfloat16), normed, preferred_element_type=jnp.float32
    ).astype(jnp.bfloat16)
    arrived = lax.all_to_all(
        outgoing.reshape(sp_ways, capacity, width), "sp", split_axis=0, concat_axis=0, tiled=True
    )
    piece = lax.all_gather(arrived.reshape(sp_ways * capacity, width), "tp", axis=0, tiled=True)
    gate = jnp.dot(piece, expert_gate[0], preferred_element_type=jnp.float32)
    upward = jnp.dot(piece, expert_up[0], preferred_element_type=jnp.float32)
    hidden = (jax.nn.silu(gate) * upward).astype(jnp.bfloat16)
    term = jnp.dot(hidden, expert_down[0], preferred_element_type=jnp.float32)
    summed = lax.psum_scatter(
        lax.optimization_barrier(term.astype(jnp.bfloat16))
        .astype(jnp.float32)
        .astype(jnp.bfloat16),
        "tp",
        scatter_dimension=0,
        tiled=True,
    )
    finished_rows = summed.reshape(sp_ways, capacity, width)
    back = lax.all_to_all(finished_rows, "sp", split_axis=0, concat_axis=0, tiled=True)
    picked = jnp.take(back.reshape(sp_ways * capacity, width), own_slots.reshape(-1), axis=0)
    picked = picked.reshape(tok_rows, top_count, width)
    output = mixed + jnp.sum(route_weights[:, :, None] * picked.astype(jnp.float32), axis=1)
    return output.astype(jnp.bfloat16)


def solution(mesh):
    placed = (
        P(("sp", "tp"), None),
        P("sp", "tp", None),
        P("sp", "tp", None),
        P("sp", "tp", None),
        P("sp", "tp", None),
        P("sp", "tp", None),
        P("sp", "tp", None),
        P("tp"),
        P("tp"),
        P(),
        P(),
        P("tp", None),
        P("tp", None),
        P(),
        P(("sp", "tp"), None),
        P(("sp", "tp"), None),
        P("sp", None, "tp"),
        P("sp", None, "tp"),
        P("sp", "tp", None),
    )
    return jax.shard_map(
        per_device, mesh=mesh, in_specs=placed, out_specs=P(("sp", "tp"), None), check_vma=False
    )
```

profile of v0, /device:TPU:11, one launch (start us, length us, event | category | flops | bytes accessed | tf_op | source)
XLA Modules:
  0.0 222.1 jit_solution(9552540781726115623)
XLA Ops:
  0.0 0.8 tile.2
  0.8 0.1 stack_tile.4
  0.9 1.4 fusion.14
  2.3 2.1 pad_maximum_fusion.1
  4.3 0.1 broadcast_in_dim.14
  4.4 0.7 maximum_multiply_fusion
  5.2 0.7 pad_maximum_fusion.par_ref
  5.9 0.8 copy.48
  6.7 0.1 eq.15
  6.8 0.1 fusion.12
  6.9 0.2 reduce_window_sum.11
  7.1 0.2 select_reduce_fusion
  7.2 0.1 reduce_sum.12
  7.5 0.7 convert_bitcast_fusion
  8.2 0.7 select_maximum_fusion
  8.9 15.7 %all-gather = f32[64,128]{1,0:T(8,128)} all-gather(f32[8,128]{1,0:T(8,128)S(1)} %select_maximum_fusion), channel_id=2, replica_groups=mesh['sp'=4,'tp'=8] {'tp'}, dimensions={0}, use_global_device_ids=true | all-gather | bytes 36864 | tf_op jit(solution)/shard_map/all_gather | solution.py:739
  24.5 1.0 copy.45.qb_ref
  25.6 1.0 copy.46.kb_ref
  26.6 1.0 copy.47.vb_ref
  27.6 1.1 copy.56
  28.7 1.1 copy_bitcast_fusion
  29.8 42.8 %shard_map.199 = bf16[4,512,128]{2,1,0:T(8,128)(2,1)S(1)} custom-call(bf16[512,256]{1,0:T(8,128)(2,1)S(1)} %bitcast.45, bf16[512,256]{1,0:T(8,128)(2,1)S(1)} %get-tuple-element.14.ka_ref, bf16[512,256]{1,0:T(8,128)(2,1)S(1)} %get-tuple-element.13.va_ref, bf16[512,128]{1,0:T(8,128)(2,1)S(1)} %copy.45.qb_ref, bf16[512,128]{1,0:T(8,128)(2,1)S(1)} %copy.46.kb_ref, ...), custom_call_target="tpu_custom_call" | custom-call | tf_op jit(solution)/shard_map/pallas_call | solution.py:293
  72.7 0.7 fusion.4
  73.4 0.3 copy-done.6
  73.7 0.7 add_convert_fusion
  74.4 0.2 copy-done.3
  74.6 69.2 %shard_map.200 = (bf16[2,4,4,48,2048]{4,3,2,1,0:T(8,128)(2,1)}, f32[64,2048]{1,0:T(8,128)S(1)}) custom-call(bf16[4,2,64,2048]{3,2,1,0:T(8,128)(2,1)S(1)} %bitcast.44, bf16[64,2048]{1,0:T(8,128)(2,1)S(1)} %copy-done.3, f32[1,2048]{1,0:T(1,128)S(1)} %bitcast.48, f32[8,8,128]{2,1,0:T(8,128)S(1)} %bitcast.47), custom_call_target="tpu_custom_call" | custom-call | tf_op jit(solution)/shard_map/pallas_call | solution.py:630
  143.9 7.8 %fusion.2 = f32[1536,768]{1,0:T(8,128)S(1)} fusion(bf16[1536,2048]{1,0:T(8,128)(2,1)} %bitcast.59, bf16[1,2048,768]{2,1,0:T(8,128)(2,1)S(1)} %copy-done.8), kind=kOutput, calls=%fused_computation.5 | convolution fusion | flops 4831838208 | bytes 14155776 | tf_op jit(solution)/shard_map/dot_general | solution.py:661
  151.7 5.6 %multiply_convert_fusion = bf16[1536,768]{1,0:T(8,128)(2,1)S(1)} fusion(f32[1536,768]{1,0:T(8,128)S(1)} %fusion.2, bf16[1536,2048]{1,0:T(8,128)(2,1)S(1)} %bitcast.60, bf16[1,2048,768]{2,1,0:T(8,128)(2,1)S(1)} %copy-done.9), kind=kOutput, calls=%fused_computation.1 | convolution fusion | flops 4838916096 | bytes 16515072 | tf_op jit(solution)/shard_map/dot_general | solution.py:662
  157.3 7.1 %convolution_convert_fusion = bf16[1536,2048]{1,0:T(8,128)(2,1)} fusion(bf16[1536,768]{1,0:T(8,128)(2,1)S(1)} %multiply_convert_fusion, bf16[1,768,2048]{2,1,0:T(8,128)(2,1)S(1)} %copy-done), kind=kOutput, calls=%fused_computation | convolution fusion | flops 4834983936 | bytes 11796480 | tf_op jit(solution)/shard_map/dot_general | solution.py:664
  164.4 56.0 %shard_map.201 = bf16[64,2048]{1,0:T(8,128)(2,1)} custom-call(bf16[2,4,4,48,2048]{4,3,2,1,0:T(8,128)(2,1)} %bitcast.49, f32[8,8,128]{2,1,0:T(8,128)} %bitcast.46, f32[64,2048]{1,0:T(8,128)} %copy-done.1), custom_call_target="tpu_custom_call" | custom-call | tf_op jit(solution)/shard_map/pallas_call | solution.py:665
  220.5 1.7 copy.58
  (20 shorter events, 0.2 us)
Async XLA Ops:
  0.0 157.3 %copy-start = (bf16[1,768,2048]{2,1,0:T(8,128)(2,1)S(1)}, bf16[1,768,2048]{2,1,0:T(8,128)(2,1)}, u32[]{:S(2)}) copy-start(bf16[1,768,2048]{2,1,0:T(8,128)(2,1)} %param.39) | copy-start | bytes 9437188
  27.6 45.0 %copy-start.5 = (bf16[256,2048]{1,0:T(8,128)(2,1)S(1)}, bf16[256,2048]{1,0:T(8,128)(2,1)}, u32[]{:S(2)}) copy-start(bf16[256,2048]{1,0:T(8,128)(2,1)} %param.32) | copy-start | bytes 3145732
  72.6 1.0 copy-start.6
  73.7 0.8 copy-start.2
  73.7 1.0 copy-start.3
  73.7 1.0 copy-start.4
  73.7 70.2 %copy-start.8 = (bf16[1,2048,768]{2,1,0:T(8,128)(2,1)S(1)}, bf16[1,2048,768]{2,1,0:T(8,128)(2,1)}, u32[]{:S(2)}) copy-start(bf16[1,2048,768]{2,1,0:T(8,128)(2,1)} %param.37) | copy-start | bytes 9437188
  143.9 7.8 %copy-start.1 = (f32[64,2048]{1,0:T(8,128)}, f32[64,2048]{1,0:T(8,128)S(1)}, u32[]{:S(2)}) copy-start(f32[64,2048]{1,0:T(8,128)S(1)} %get-tuple-element.8.mixed_ref) | copy-start | bytes 1572868
  143.9 7.8 %copy-start.7 = (bf16[2,4,4,48,2048]{4,3,2,1,0:T(8,128)(2,1)S(1)}, bf16[2,4,4,48,2048]{4,3,2,1,0:T(8,128)(2,1)}, u32[]{:S(2)}) copy-start(bf16[2,4,4,48,2048]{4,3,2,1,0:T(8,128)(2,1)} %get-tuple-element.7) | copy-start | bytes 18874372
  143.9 7.8 %copy-start.9 = (bf16[1,2048,768]{2,1,0:T(8,128)(2,1)S(1)}, bf16[1,2048,768]{2,1,0:T(8,128)(2,1)}, u32[]{:S(2)}) copy-start(bf16[1,2048,768]{2,1,0:T(8,128)(2,1)} %param.38) | copy-start | bytes 9437188
where the time goes:
time: 226 us; the launch traced here: 222 us
  Pallas kernels  168 us (74%)
  matrix products  21.9 us (10%)
  blocking collectives  15.7 us (7%)
  local copies, waits for them, and re-layouts  11 us (5%)
  other arithmetic  5.35 us (2%)
    pallas_call x1, Pallas kernels, routed_experts(): pl.pallas_call(functools.partial(dispatch_kernel, places, chips, capacity...  69.2 us
    pallas_call x1, Pallas kernels, routed_experts(): pl.pallas_call(functools.partial(combine_kernel, places, chips, capacity)...  56 us
    pallas_call x1, Pallas kernels, whole_heads(): pl.pallas_call(functools.partial(heads_kernel, order, chunk), out_shape=j...  42.8 us
    all_gather x1, blocking collectives, per_device(): meta = lax.all_gather(meta, 'tp', axis=0)  15.7 us
    dot_general x1, matrix products, routed_experts(): gate = jnp.dot(piece, expert_gate[0], preferred_element_type=jnp.float32)  7.79 us
    dot_general x1, matrix products, routed_experts(): term = jnp.dot(hidden, expert_down[0], preferred_element_type=jnp.float32)  7.07 us
    dot_general x1, matrix products, routed_experts(): upward = jnp.dot(piece, expert_up[0], preferred_element_type=jnp.float32)  5.59 us

commit v1 on v0

--- a/solution.py
+++ b/solution.py
@@ -399,22 +399,72 @@
     pl.semaphore_wait(barrier, len(peers))
 
 
-def dispatch_kernel(
+def flipped(value, apart):
+    bit = 1
+    while bit <= apart:
+        if apart & bit:
+            value = value + bit - 2 * bit * lax.rem(lax.div(value, bit), 2)
+        bit *= 2
+    return value
+
+
+def route_table(ids, weights, cap):
+    rows = ids.shape[0]
+    lane = lax.broadcasted_iota(jnp.int32, (rows, 128), 1)
+    hits = [ids[:, which : which + 1] == lane for which in range(2)]
+    named = jnp.where(hits[0], 1.0, 0.0) + jnp.where(hits[1], 1.0, 0.0)
+    above = lax.broadcasted_iota(jnp.int32, (rows, rows), 0)
+    above = above > lax.broadcasted_iota(jnp.int32, (rows, rows), 1)
+    ranks = jnp.dot(
+        jnp.where(above, 1.0, 0.0).astype(jnp.bfloat16),
+        named.astype(jnp.bfloat16),
+        preferred_element_type=jnp.float32,
+    )
+    spots = ranks + (lane * cap).astype(jnp.float32)
+    table = jnp.zeros((rows, 128), jnp.float32)
+    for which in range(2):
+        spot = jnp.sum(jnp.where(hits[which], spots, 0.0), axis=1, keepdims=True)
+        table = jnp.where(lane == which, spot, table)
+        table = jnp.where(lane == which + 2, weights[:, which : which + 1], table)
+    table = jnp.concatenate([table, jnp.zeros((128 - rows, 128), jnp.float32)], axis=0)
+    return table.T[0:8, :]
+
+
+def experts_kernel(
     places,
     chips,
     cap,
     term_ref,
     resid_ref,
     gain_ref,
-    meta_ref,
+    ids_ref,
+    weights_ref,
+    gate_hbm,
+    up_hbm,
+    down_hbm,
     out_ref,
-    mixed_ref,
-    normed_ref,
+    gate,
+    up,
+    down,
+    table,
+    mixed,
+    normed,
     twin,
     chip_sum,
     sums,
     near,
     stage,
+    piece,
+    hidden,
+    part,
+    pair,
+    finished,
+    back,
+    leave,
+    last,
+    ws,
+    ms,
+    mr,
     ts,
     tr,
     rs,
@@ -425,194 +475,212 @@
     xr,
     ps,
     pr,
+    qs,
+    qr,
+    bs,
+    br,
+    ls,
+    lr,
 ):
     place, turn = lax.axis_index("sp"), lax.axis_index("tp")
     chip, core = lax.div(turn, 2), lax.rem(turn, 2)
     other = 2 * chip + 1 - core
-    rows = normed_ref.shape[0]
+    rows, width = normed.shape
+    slots = places * cap
+    loads = [
+        pltpu.make_async_copy(src, dst, ws.at[at])
+        for at, (src, dst) in enumerate(((gate_hbm, gate), (up_hbm, up), (down_hbm, down)))
+    ]
+    for load in loads:
+        load.start()
+    table[0] = route_table(ids_ref[...], weights_ref[...], cap)
     greet_routes(places, chips)
+    others = list(range(1, chips))
+
+    def peer(apart):
+        return 2 * flipped(chip, apart) + core
+
+    def table_copy(apart):
+        return remote(
+            table.at[0], table.at[apart], ms.at[apart], mr.at[apart], tp=peer(apart)
+        )
 
     def twin_copy(apart):
-        spot = term_ref.at[lax.rem(chip + apart, chips), 1 - core]
+        spot = term_ref.at[flipped(chip, apart), 1 - core]
         return remote(spot, twin.at[apart], ts.at[apart], tr.at[apart], tp=other)
 
     def sum_copy(apart):
-        peer = 2 * lax.rem(chip + apart, chips) + core
-        return remote(chip_sum.at[apart], sums.at[apart], rs.at[apart], rr.at[apart], tp=peer)
-
-    turns = list(range(1, chips)) + [0]
+        return remote(
+            chip_sum.at[apart], sums.at[apart], rs.at[apart], rr.at[apart], tp=peer(apart)
+        )
+
+    def near_copy(apart):
+        return remote(normed, near.at[apart], zs.at[apart], zr.at[apart], tp=peer(apart))
+
+    def route_copy(apart, away):
+        expert = flipped(place, away)
+        return remote(
+            stage.at[apart, expert],
+            piece.at[apart, core, place],
+            xs.at[apart, away],
+            xr.at[apart, away],
+            sp=expert,
+        )
+
+    def pair_copy(apart):
+        spot = piece.at[apart, core]
+        return remote(spot, spot, ps.at[apart], pr.at[apart], tp=other)
+
+    def part_copy(apart):
+        return remote(
+            part.at[apart, 1 - core], pair.at[apart], qs.at[apart], qr.at[apart], tp=other
+        )
+
+    def back_copy(apart, away):
+        home = flipped(place, away)
+        return remote(
+            finished.at[apart, home],
+            back.at[apart, place],
+            bs.at[apart, away],
+            br.at[apart, away],
+            sp=home,
+        )
+
+    def last_copy(apart):
+        return remote(leave.at[apart], last.at[apart], ls.at[apart], lr.at[apart], tp=peer(apart))
+
+    turns = list(reversed(others)) + [0]
     for apart in turns:
         twin_copy(apart).start()
+    for apart in others:
+        table_copy(apart).start()
     total = resid_ref[...].astype(jnp.float32)
     for apart in turns:
         twin_copy(apart).wait_recv()
-        both = term_ref[lax.rem(chip + apart, chips), core].astype(jnp.float32) + twin[
-            apart
-        ].astype(jnp.float32)
+        both = term_ref[flipped(chip, apart), core].astype(jnp.float32)
+        both = both + twin[apart].astype(jnp.float32)
         if apart:
             chip_sum[apart] = both.astype(jnp.bfloat16)
             sum_copy(apart).start()
         else:
             total = total + both
-    for apart in range(1, chips):
+    for apart in others:
         sum_copy(apart).wait_recv()
         total = total + sums[apart].astype(jnp.float32)
-    mixed_ref[...] = total
-    normed_ref[...] = rms_scaled(total, gain_ref[...]).astype(jnp.bfloat16)
-
-    def near_copy(apart):
-        peer = 2 * lax.rem(chip + apart, chips) + core
-        return remote(normed_ref, near.at[apart], zs.at[apart], zr.at[apart], tp=peer)
-
-    for apart in range(1, chips):
+    mixed[...] = total
+    normed[...] = rms_scaled(total, gain_ref[...]).astype(jnp.bfloat16)
+    for apart in others:
         near_copy(apart).start()
 
-    def source(apart):
-        return lax.rem(chip + chips - apart, chips)
-
-    def route_copy(apart, away):
-        expert = lax.rem(place + away, places)
-        return remote(
-            stage.at[apart, expert],
-            out_ref.at[core, source(apart), place],
-            xs.at[apart, away],
-            xr.at[apart, away],
-            sp=expert,
-        )
-
-    def pair_copy(apart, away):
-        spot = out_ref.at[core, source(apart), lax.rem(place + places - away, places)]
-        return remote(spot, spot, ps.at[apart, away], pr.at[apart, away], tp=other)
-
-    slot = lax.broadcasted_iota(jnp.int32, (places * cap, rows), 0).astype(jnp.float32)
-    for apart in range(chips):
-        owner = 2 * source(apart) + core
-        spread = jnp.zeros((places * cap, rows), jnp.float32)
+    slot = lax.broadcasted_iota(jnp.int32, (rows, slots), 1).astype(jnp.float32)
+
+    def columns(apart):
+        full = jnp.concatenate([table[apart], jnp.zeros((120, 128), jnp.float32)], axis=0)
+        return full.T[0:rows, :]
+
+    def send_out(apart):
+        if apart:
+            table_copy(apart).wait_recv()
+            near_copy(apart).wait_recv()
+        held = near[apart] if apart else normed[...]
+        known = columns(apart)
+        spread = jnp.zeros((rows, slots), jnp.float32)
         for which in range(2):
-            own = meta_ref[owner, which : which + 1, 0:rows]
-            spread = spread + jnp.where(slot == own, 1.0, 0.0)
-        if apart:
-            near_copy(apart).wait_recv()
-            piece = near[apart]
-        else:
-            piece = normed_ref[...]
-        sent = jnp.dot(spread.astype(jnp.bfloat16), piece, preferred_element_type=jnp.float32)
-        stage[apart] = sent.astype(jnp.bfloat16).reshape(places, cap, sent.shape[1])
-        for away in range(1, places):
+            spread = spread + jnp.where(slot == known[:, which : which + 1], 1.0, 0.0)
+        sent = lax.dot_general(
+            spread.astype(jnp.bfloat16),
+            held,
+            (((0,), (0,)), ((), ())),
+            preferred_element_type=jnp.float32,
+        )
+        stage[apart] = sent.astype(jnp.bfloat16).reshape(places, cap, width)
+        for away in reversed(range(1, places)):
             route_copy(apart, away).start()
-        out_ref[core, source(apart), place] = stage[apart, place]
-        pair_copy(apart, 0).start()
-    for apart in range(chips):
+        piece[apart, core, place] = stage[apart, place]
+
+    def run_expert(apart):
         for away in range(1, places):
             route_copy(apart, away).wait_recv()
-            pair_copy(apart, away).start()
-    for apart in range(chips):
-        twin_copy(apart).wait_send()
+        pair_copy(apart).start()
+        pair_copy(apart).wait_recv()
+        tile = 256
+
+        @pl.loop(0, hidden.shape[1] // tile)
+        def _(step):
+            cols = pl.ds(pl.multiple_of(step * tile, tile), tile)
+            given = piece[apart].reshape(2 * slots, width)
+            opened = jnp.dot(given, gate[:, cols], preferred_element_type=jnp.float32)
+            raised = jnp.dot(given, up[:, cols], preferred_element_type=jnp.float32)
+            hidden[:, cols] = (jax.nn.silu(opened) * raised).astype(jnp.bfloat16)
+
+        wide = 512
+
+        @pl.loop(0, width // wide)
+        def _(step):
+            cols = pl.ds(pl.multiple_of(step * wide, wide), wide)
+            lowered = jnp.dot(hidden[...], down[:, cols], preferred_element_type=jnp.float32)
+            part[apart, :, :, cols] = lowered.astype(jnp.bfloat16).reshape(2, slots, wide)
+
+        part_copy(apart).start()
+
+    def settle(apart):
+        part_copy(apart).wait_recv()
+        both = part[apart, core].astype(jnp.float32) + pair[apart].astype(jnp.float32)
+        finished[apart] = both.astype(jnp.bfloat16).reshape(places, cap, width)
         if apart:
-            sum_copy(apart).wait_send()
-            near_copy(apart).wait_send()
-        for away in range(places):
-            if away:
-                route_copy(apart, away).wait_send()
-            pair_copy(apart, away).wait()
-
-
-def combine_kernel(
-    places,
-    chips,
-    cap,
-    term_ref,
-    meta_ref,
-    mixed_ref,
-    out_ref,
-    pair,
-    stage,
-    back,
-    leave,
-    near,
-    ps,
-    pr,
-    xs,
-    xr,
-    zs,
-    zr,
-):
-    place, turn = lax.axis_index("sp"), lax.axis_index("tp")
-    chip, core = lax.div(turn, 2), lax.rem(turn, 2)
-    other = 2 * chip + 1 - core
-    rows = mixed_ref.shape[0]
-    greet_routes(places, chips)
-    order = list(range(1, chips)) + [0]
-
-    def source(apart):
-        return lax.rem(chip + chips - apart, chips)
-
-    def pair_copy(apart):
-        return remote(
-            term_ref.at[1 - core, source(apart)],
-            pair.at[apart],
-            ps.at[apart],
-            pr.at[apart],
-            tp=other,
-        )
-
-    def back_copy(apart, away):
-        peer = lax.rem(place + away, places)
-        return remote(
-            stage.at[apart, peer],
-            back.at[apart, place],
-            xs.at[apart, away],
-            xr.at[apart, away],
-            sp=peer,
-        )
-
-    def near_copy(apart):
-        peer = 2 * source(apart) + core
-        return remote(leave.at[apart], near.at[apart], zs.at[apart], zr.at[apart], tp=peer)
-
-    for apart in order:
-        pair_copy(apart).start()
-    for apart in order:
-        pair_copy(apart).wait_recv()
-        for expert in range(places):
-            stage[apart, expert] = (
-                term_ref[core, source(apart), expert].astype(jnp.float32)
-                + pair[apart, expert].astype(jnp.float32)
-            ).astype(jnp.bfloat16)
-        for away in range(1, places):
+            send_back(apart)
+
+    def send_back(apart):
+        for away in reversed(range(1, places)):
             back_copy(apart, away).start()
-        back[apart, place] = stage[apart, place]
-    slot = lax.broadcasted_iota(jnp.int32, (places * cap, rows), 0).astype(jnp.float32)
-    total = mixed_ref[...]
-    for apart in order:
-        owner = 2 * source(apart) + core
-        gather = jnp.zeros((places * cap, rows), jnp.float32)
+        back[apart, place] = finished[apart, place]
+
+    def gathered(apart):
+        known = columns(apart)
+        gather = jnp.zeros((rows, slots), jnp.float32)
         for which in range(2):
-            own = meta_ref[owner, which : which + 1, 0:rows]
-            weight = meta_ref[owner, which + 2 : which + 3, 0:rows]
-            gather = gather + jnp.where(slot == own, weight, 0.0)
+            own = known[:, which : which + 1]
+            gather = gather + jnp.where(slot == own, known[:, which + 2 : which + 3], 0.0)
         high = gather.astype(jnp.bfloat16)
         low = (gather - high.astype(jnp.float32)).astype(jnp.bfloat16)
         for away in range(1, places):
             back_copy(apart, away).wait_recv()
-        held = back[apart].reshape(places * cap, back.shape[3])
-        dims = (((0,), (0,)), ((), ()))
-        part = lax.dot_general(high, held, dims, preferred_element_type=jnp.float32)
-        part = part + lax.dot_general(low, held, dims, preferred_element_type=jnp.float32)
+        held = back[apart].reshape(slots, width)
+        found = jnp.dot(high, held, preferred_element_type=jnp.float32)
+        return found + jnp.dot(low, held, preferred_element_type=jnp.float32)
+
+    ahead = min(3, chips)
+    for apart in range(ahead):
+        send_out(apart)
+    for load in loads:
+        load.wait()
+    for apart in range(chips):
+        run_expert(apart)
+        if apart + ahead < chips:
+            send_out(apart + ahead)
         if apart:
-            leave[apart] = part.astype(jnp.bfloat16)
-            near_copy(apart).start()
-        else:
-            total = total + part
-    for apart in range(1, chips):
-        near_copy(apart).wait_recv()
-        total = total + near[apart].astype(jnp.float32)
+            settle(apart - 1)
+    settle(chips - 1)
+    send_back(0)
+    for apart in others:
+        leave[apart] = gathered(apart).astype(jnp.bfloat16)
+        last_copy(apart).start()
+    total = mixed[...] + gathered(0)
+    for apart in others:
+        last_copy(apart).wait_recv()
+        total = total + last[apart].astype(jnp.float32)
     out_ref[...] = total.astype(jnp.bfloat16)
     for apart in range(chips):
+        twin_copy(apart).wait_send()
+        pair_copy(apart).wait_send()
+        part_copy(apart).wait_send()
         if apart:
+            table_copy(apart).wait_send()
+            sum_copy(apart).wait_send()
             near_copy(apart).wait_send()
-        pair_copy(apart).wait_send()
+            last_copy(apart).wait_send()
         for away in range(1, places):
+            route_copy(apart, away).wait_send()
             back_copy(apart, away).wait_send()
 
 
@@ -620,70 +688,63 @@
     return [pl.BlockSpec(memory_space=pltpu.VMEM)] * count
 
 
-def routed_experts(term, resid, norm_gain, meta, capacity, expert_gate, expert_up, expert_down):
+def routed_experts(
+    term, resid, norm_gain, route_ids, route_weights, capacity, gate, upward, down
+):
     places, chips = lax.axis_size("sp"), lax.axis_size("tp") // 2
     rows, width = resid.shape
-    shape = (2, chips, places, capacity, width)
+    deep = gate.shape[2]
+    slots = places * capacity
     sems = pltpu.SemaphoreType.DMA
-    half = pltpu.VMEM((chips, places, capacity, width), jnp.bfloat16)
-    piece_rows = pltpu.VMEM((chips, rows, width), jnp.bfloat16)
-    piece, mixed = pl.pallas_call(
-        functools.partial(dispatch_kernel, places, chips, capacity),
-        out_shape=(
-            jax.ShapeDtypeStruct(shape, jnp.bfloat16),
-            jax.ShapeDtypeStruct((rows, width), jnp.float32),
-        ),
-        in_specs=vmem(4),
-        out_specs=vmem(2),
+
+    def held(*shape):
+        return pltpu.VMEM(shape, jnp.bfloat16)
+
+    return pl.pallas_call(
+        functools.partial(experts_kernel, places, chips, capacity),
+        out_shape=jax.ShapeDtypeStruct((rows, width), jnp.bfloat16),
+        in_specs=vmem(5) + [pl.BlockSpec(memory_space=pl.ANY)] * 3,
+        out_specs=vmem(1)[0],
         scratch_shapes=[
-            pltpu.VMEM((rows, width), jnp.bfloat16),
-            piece_rows,
-            piece_rows,
-            piece_rows,
-            piece_rows,
-            half,
-            sems((chips,)),
-            sems((chips,)),
-            sems((chips,)),
-            sems((chips,)),
-            sems((chips,)),
-            sems((chips,)),
-            sems((chips, places)),
-            sems((chips, places)),
-            sems((chips, places)),
-            sems((chips, places)),
+            held(width, deep),
+            held(width, deep),
+            held(deep, width),
+            pltpu.VMEM((chips, 8, 128), jnp.float32),
+            pltpu.VMEM((rows, width), jnp.float32),
+            held(rows, width),
+            held(chips, rows, width),
+            held(chips, rows, width),
+            held(chips, rows, width),
+            held(chips, rows, width),
+            held(chips, places, capacity, width),
+            held(chips, 2, places, capacity, width),
+            held(2 * slots, deep),
+            held(chips, 2, slots, width),
+            held(chips, slots, width),
+            held(chips, places, capacity, width),
+            held(chips, places, capacity, width),
+            held(chips, rows, width),
+            held(chips, rows, width),
+            sems((3,)),
+            *[sems((chips,))] * 8,
+            *[sems((chips, places))] * 2,
+            *[sems((chips,))] * 4,
+            *[sems((chips, places))] * 2,
+            *[sems((chips,))] * 2,
         ],
         compiler_params=pltpu.CompilerParams(
-            collective_id=2, has_side_effects=True, vmem_limit_bytes=48 << 20
+            collective_id=2, has_side_effects=True, vmem_limit_bytes=60 << 20
         ),
-    )(term.reshape(chips, 2, rows, width), resid, norm_gain[None, :], meta)
-    piece = piece.reshape(-1, width)
-    gate = jnp.dot(piece, expert_gate[0], preferred_element_type=jnp.float32)
-    upward = jnp.dot(piece, expert_up[0], preferred_element_type=jnp.float32)
-    hidden = (jax.nn.silu(gate) * upward).astype(jnp.bfloat16)
-    term = jnp.dot(hidden, expert_down[0], preferred_element_type=jnp.float32)
-    return pl.pallas_call(
-        functools.partial(combine_kernel, places, chips, capacity),
-        out_shape=jax.ShapeDtypeStruct((rows, width), jnp.bfloat16),
-        in_specs=vmem(3),
-        out_specs=vmem(1)[0],
-        scratch_shapes=[
-            half,
-            half,
-            half,
-            piece_rows,
-            piece_rows,
-            sems((chips,)),
-            sems((chips,)),
-            sems((chips, places)),
-            sems((chips, places)),
-            sems((chips,)),
-            sems((chips,)),
-        ],
-        compiler_params=pltpu.CompilerParams(
-            collective_id=3, has_side_effects=True, vmem_limit_bytes=56 << 20
-        ),
-    )(term.astype(jnp.bfloat16).reshape(shape), meta, mixed)
+    )(
+        term.reshape(chips, 2, rows, width),
+        resid,
+        norm_gain[None, :],
+        route_ids,
+        route_weights,
+        gate[0],
+        upward[0],
+        down[0],
+    )
 
 
 def per_device(
@@ -729,24 +790,23 @@
     tok_rows = resid.shape[0]
     top_count = route_ids.shape[1]
     capacity = 3 * top_count * tok_rows // (2 * sp_ways)
-    own_slots = slot_numbers(route_ids, sp_ways, capacity)
     term = jnp.dot(heads_out_a, proj_a, preferred_element_type=jnp.float32)
     term = term + jnp.dot(heads_out_b, proj_b, preferred_element_type=jnp.float32)
     tp_ways = lax.axis_size("tp")
-    if top_count == 2 and capacity % 16 == 0 and tok_rows <= 128 and tp_ways % 2 == 0:
-        meta = jnp.concatenate([own_slots.astype(jnp.float32).T, route_weights.T], axis=0)
-        meta = jnp.pad(meta, ((0, 4), (0, 128 - tok_rows)))
-        meta = lax.all_gather(meta, "tp", axis=0)
+    paired = tp_ways % 2 == 0 and tp_ways & (tp_ways - 1) == 0 and sp_ways & (sp_ways - 1) == 0
+    if paired and top_count == 2 and capacity % 16 == 0 and tok_rows <= 128:
         return routed_experts(
             term.astype(jnp.bfloat16),
             resid,
             norm_gain,
-            meta,
+            route_ids,
+            route_weights,
             capacity,
             expert_gate,
             expert_up,
             expert_down,
         )
+    own_slots = slot_numbers(route_ids, sp_ways, capacity)
     mixed = resid.astype(jnp.float32) + lax.psum_scatter(
         lax.optimization_barrier(term.astype(jnp.bfloat16))
         .astype(jnp.float32)

time: 226 us -> 177 us (0.78); the launches traced: 222 us -> 176 us
  matrix products: 21.9 us -> 2.78 us
  blocking collectives: 15.7 us -> 0 us
  Pallas kernels: 168 us -> 159 us
    dot_general x3 -> x0, matrix products: 20.4 us -> none  [the longest x1 7.79 us: routed_experts(): gate = jnp.dot(piece, expert_gate[0], preferred_element_type=jnp.float32)]
    all_gather x1 -> x0, blocking collectives: 15.7 us -> none  [per_device(): meta = lax.all_gather(meta, 'tp', axis=0)]
    pallas_call x2 -> x1, Pallas kernels: 125 us -> 117 us  [routed_experts(): pl.pallas_call(functools.partial(experts_kernel, places, chips, capacity)...]
where the time goes in v1:
time: 177 us; the launch traced here: 176 us
  Pallas kernels  159 us (90%)
  local copies, waits for them, and re-layouts  10.8 us (6%)
  other arithmetic  3.53 us (2%)
  matrix products  2.78 us (2%)
    pallas_call x1, Pallas kernels, routed_experts(): pl.pallas_call(functools.partial(experts_kernel, places, chips, capacity)...  117 us
    pallas_call x1, Pallas kernels, whole_heads(): pl.pallas_call(functools.partial(heads_kernel, order, chunk), out_shape=j...  42 us
    unnamed x12, local copies, waits for them, and re-layouts  4.37 us

profile of v1, /device:TPU:11, one launch (start us, length us, event | category | flops | bytes accessed | tf_op | source)
XLA Modules:
  0.0 176.1 jit_solution(16790831535340611679)
XLA Ops:
  0.0 0.0 copy-start
  0.0 1.4 fusion.9
  1.4 2.1 %pad_maximum_fusion.1 = f32[4]{0:T(128)S(1)} fusion(f32[1]{0:T(128)} %get-tuple-element.8, f32[2]{0:T(128)} %param.29, f32[1]{0:T(128)} %get-tuple-element.7), kind=kLoop, calls=%fused_computation.16 | loop fusion | flops 8 | bytes 32 | tf_op jit(solution)/shard_map/stack | solution.py:282
  3.5 0.1 broadcast_in_dim.13
  3.6 0.7 tile.2
  4.2 0.1 stack_tile.4
  4.3 0.7 maximum_multiply_fusion
  5.0 0.7 pad_maximum_fusion.par_ref
  5.8 1.1 copy_bitcast_fusion
  6.9 1.0 copy.38
  7.9 1.0 copy.27.qb_ref
  8.9 1.0 copy.28.kb_ref
  9.9 1.0 copy.29.vb_ref
  11.0 42.0 %shard_map.199 = bf16[4,512,128]{2,1,0:T(8,128)(2,1)S(1)} custom-call(bf16[512,256]{1,0:T(8,128)(2,1)S(1)} %bitcast.29, bf16[512,256]{1,0:T(8,128)(2,1)S(1)} %get-tuple-element.10.ka_ref, bf16[512,256]{1,0:T(8,128)(2,1)S(1)} %get-tuple-element.9.va_ref, bf16[512,128]{1,0:T(8,128)(2,1)S(1)} %copy.27.qb_ref, bf16[512,128]{1,0:T(8,128)(2,1)S(1)} %copy.28.kb_ref, ...), custom_call_target="tpu_custom_call" | custom-call | tf_op jit(solution)/shard_map/pallas_call | solution.py:293
  53.0 0.0 copy-start.1
  53.0 0.0 copy-done
  53.0 0.7 fusion
  53.8 0.3 copy-done.1
  54.0 0.0 copy-start.2
  54.0 0.0 copy-start.3
  54.0 2.1 %add_convert_fusion = bf16[512,2048]{1,0:T(8,128)(2,1)} fusion(f32[512,2048]{1,0:T(8,128)S(1)} %fusion, bf16[128,2048]{1,0:T(8,128)(2,1)S(1)} %copy-done.1, bf16[4,512,128]{2,1,0:T(8,128)(2,1)S(1)} %shard_map.199), kind=kOutput, calls=%fused_computation | convolution fusion | flops 270598144 | bytes 7077888 | tf_op jit(solution)/shard_map/dot_general | solution.py:794
  56.1 0.0 copy-done.2
  56.1 0.7 copy.30.ids_ref
  56.8 0.0 copy-done.3
  56.8 0.7 copy.31.weights_ref
  57.5 116.9 %shard_map.200 = bf16[64,2048]{1,0:T(8,128)(2,1)} custom-call(bf16[4,2,64,2048]{3,2,1,0:T(8,128)(2,1)} %bitcast.30, bf16[64,2048]{1,0:T(8,128)(2,1)} %resid_ref.1, f32[1,2048]{1,0:T(1,128)} %bitcast.41, s32[64,2]{1,0:T(8,128)} %copy.30.ids_ref, f32[64,2]{1,0:T(8,128)} %copy.31.weights_ref, bf16[2048,768]{1,0:T(8,128)(2,1)} %bitcast.31, ...), custom_call_target="tpu_custom_call" | custom-call | tf_op jit(solution)/shard_map/pallas_call | solution.py:703
  174.4 1.7 copy.40
  (1 shorter events, 0.0 us)
Async XLA Ops:
  0.0 53.0 %copy-start = (bf16[256,2048]{1,0:T(8,128)(2,1)S(1)}, bf16[256,2048]{1,0:T(8,128)(2,1)}, u32[]{:S(2)}) copy-start(bf16[256,2048]{1,0:T(8,128)(2,1)} %param.32) | copy-start | bytes 3145732
  53.0 1.0 copy-start.1
  54.0 2.1 %copy-start.2 = (s32[64,2]{0,1:T(2,128)S(1)}, s32[64,2]{0,1:T(2,128)}, u32[]{:S(2)}) copy-start(s32[64,2]{0,1:T(2,128)} %param.35) | copy-start | bytes 1540
  54.0 2.8 %copy-start.3 = (f32[64,2]{0,1:T(2,128)S(1)}, f32[64,2]{0,1:T(2,128)}, u32[]{:S(2)}) copy-start(f32[64,2]{0,1:T(2,128)} %param.36) | copy-start | bytes 1540

commit v2 on v1

--- a/solution.py
+++ b/solution.py
@@ -3,7 +3,6 @@
 
 import jax
 import jax.numpy as jnp
-import numpy as np
 from jax import lax
 from jax.experimental import pallas as pl
 from jax.experimental.pallas import tpu as pltpu
@@ -113,215 +112,6 @@
     return normed.astype(jnp.bfloat16).reshape(mixed.shape[0], -1)
 
 
-def greet(axis, ways):
-    me = lax.axis_index(axis)
-    barrier = pltpu.get_barrier_semaphore()
-    for apart in range(1, ways):
-        pl.semaphore_signal(
-            barrier,
-            inc=1,
-            device_id={axis: lax.rem(me + apart, ways)},
-            device_id_type=pl.DeviceIdType.MESH,
-        )
-    pl.semaphore_wait(barrier, ways - 1)
-
-
-def heads_kernel(
-    units,
-    chunk,
-    qa_ref,
-    ka_ref,
-    va_ref,
-    qb_ref,
-    kb_ref,
-    vb_ref,
-    par_ref,
-    out_ref,
-    got_q,
-    got_k,
-    got_v,
-    heads,
-    send_in,
-    recv_in,
-    send_out,
-    recv_out,
-):
-    me = lax.axis_index("sp")
-    ways, rows, wide = got_q.shape
-    greet("sp", ways)
-    refs = {"a": (qa_ref, ka_ref, va_ref), "b": (qb_ref, kb_ref, vb_ref)}
-
-    def unit_source(unit, kind):
-        group, head = units[unit]
-        ref = refs[group][kind]
-        return ref.at[:, head * wide : (head + 1) * wide] if group == "a" else ref
-
-    def unit_copy(unit, kind, landing, slot):
-        return pltpu.make_async_remote_copy(
-            src_ref=unit_source(unit, kind),
-            dst_ref=(got_q, got_k, got_v)[kind].at[landing],
-            send_sem=send_in.at[kind, unit],
-            recv_sem=recv_in.at[kind, slot],
-            device_id={"sp": unit},
-            device_id_type=pl.DeviceIdType.MESH,
-        )
-
-    for unit in range(ways):
-
-        @pl.when(me != unit)
-        def _():
-            for kind in range(3):
-                unit_copy(unit, kind, me, me).start()
-
-        @pl.when(me == unit)
-        def _():
-            for kind in range(3):
-                (got_q, got_k, got_v)[kind][unit] = unit_source(unit, kind)[...]
-
-    for unit in range(ways):
-
-        @pl.when(me != unit)
-        def _():
-            for kind in range(3):
-                unit_copy(unit, kind, unit, unit).wait()
-
-    par = par_ref[me]
-    gain, mix = par[0:1, :], par[1:2, :]
-    scale, share = par[2:3, 0:1], par[3:4, 0:1]
-    valid = par[6:7, :]
-
-    def result_copy(block):
-        return pltpu.make_async_remote_copy(
-            src_ref=heads.at[block],
-            dst_ref=out_ref.at[me],
-            send_sem=send_out.at[block],
-            recv_sem=recv_out.at[me],
-            device_id={"sp": block},
-            device_id_type=pl.DeviceIdType.MESH,
-        )
-
-    for block in reversed(range(ways)):
-        length = (block + 1) * rows
-
-        @pl.loop(0, rows // chunk)
-        def _(step):
-            first = pl.multiple_of(step * chunk, chunk)
-            query = got_q[block, pl.ds(first, chunk), :]
-            keys = got_k[0 : block + 1].reshape(length, wide)
-            values = got_v[0 : block + 1].reshape(length, wide)
-            row = first + block * rows + lax.broadcasted_iota(jnp.int32, (chunk, rows), 0)
-            col = block * rows + lax.broadcasted_iota(jnp.int32, (chunk, rows), 1)
-            parts = []
-            for which in range(2):
-                picked = query * par[4 + which : 5 + which, :].astype(jnp.bfloat16)
-                scores = lax.dot_general(
-                    picked, keys, (((1,), (1,)), ((), ())), preferred_element_type=jnp.float32
-                )
-                last = jnp.where(col <= row, scores[:, block * rows :], NEG)
-                if block:
-                    scores = jnp.concatenate([scores[:, : block * rows], last], axis=1)
-                else:
-                    scores = last
-                top = jnp.max(scores, axis=1, keepdims=True)
-                weights = jnp.exp2((scores - top) * scale)
-                sums = jnp.sum(weights, axis=1, keepdims=True)
-                mixed = jnp.dot(
-                    weights.astype(jnp.bfloat16), values, preferred_element_type=jnp.float32
-                )
-                parts.append(mixed / sums)
-            mixed = parts[0] - mix * parts[1]
-            square = jnp.sum(mixed * mixed * valid, axis=1, keepdims=True) * share
-            heads[block, pl.ds(first, chunk), :] = (
-                mixed * lax.rsqrt(square + EPS) * gain * HEAD_SCALE
-            ).astype(jnp.bfloat16)
-
-        @pl.when(me != block)
-        def _():
-            result_copy(block).start()
-
-        @pl.when(me == block)
-        def _():
-            out_ref[block] = heads[block]
-
-    for block in range(ways):
-
-        @pl.when(me != block)
-        def _():
-            result_copy(block).wait_send()
-            pltpu.make_async_remote_copy(
-                src_ref=heads.at[block],
-                dst_ref=out_ref.at[block],
-                send_sem=send_out.at[block],
-                recv_sem=recv_out.at[block],
-                device_id={"sp": block},
-                device_id_type=pl.DeviceIdType.MESH,
-            ).wait_recv()
-
-
-def whole_heads(query_a, key_a, value_a, query_b, key_b, value_b, mix_a, mix_b, gain_a, gain_b):
-    ways = lax.axis_size("sp")
-    heads_a, heads_b = query_a.shape[1], query_b.shape[1]
-    rows, wide = query_a.shape[0], value_a.shape[2]
-    order = [("a", h) for h in range(heads_a)]
-    spot = heads_a // 2
-    order = order[:spot] + [("b", h) for h in range(heads_b)] + order[spot:]
-    fixed = np.zeros((ways, 8, wide), np.float32)
-    for unit, (group, head) in enumerate(order):
-        value_wide = value_a.shape[2] if group == "a" else value_b.shape[2]
-        narrow = (query_a.shape[2] if group == "a" else query_b.shape[2]) // 2
-        first = 0 if group == "a" else head * 2 * narrow
-        fixed[unit, 2] = math.log2(math.e) / math.sqrt(narrow)
-        fixed[unit, 3] = 1.0 / value_wide
-        fixed[unit, 4, first : first + narrow] = 1.0
-        fixed[unit, 5, first + narrow : first + 2 * narrow] = 1.0
-        first = 0 if group == "a" else head * value_wide
-        fixed[unit, 6, first : first + value_wide] = 1.0
-    gains = jnp.stack(
-        [gain_a if group == "a" else jnp.tile(gain_b, heads_b) for group, _ in order]
-    )
-    mixes = jnp.stack([(mix_a if group == "a" else mix_b)[head] for group, head in order])
-    par = jnp.concatenate(
-        [
-            (gains * fixed[:, 6])[:, None, :],
-            jnp.broadcast_to(mixes[:, None, None], (ways, 1, wide)),
-            fixed[:, 2:],
-        ],
-        axis=1,
-    )
-    chunk = math.gcd(rows, 128)
-    held = pltpu.VMEM((ways, rows, wide), jnp.bfloat16)
-    got = pl.pallas_call(
-        functools.partial(heads_kernel, order, chunk),
-        out_shape=jax.ShapeDtypeStruct((ways, rows, wide), jnp.bfloat16),
-        in_specs=[pl.BlockSpec(memory_space=pltpu.VMEM)] * 7,
-        out_specs=pl.BlockSpec(memory_space=pltpu.VMEM),
-        scratch_shapes=[
-            held,
-            held,
-            held,
-            held,
-            pltpu.SemaphoreType.DMA((3, ways)),
-            pltpu.SemaphoreType.DMA((3, ways)),
-            pltpu.SemaphoreType.DMA((ways,)),
-            pltpu.SemaphoreType.DMA((ways,)),
-        ],
-        compiler_params=pltpu.CompilerParams(
-            collective_id=1, has_side_effects=True, vmem_limit_bytes=48 << 20
-        ),
-    )(
-        query_a.reshape(rows, -1),
-        key_a.reshape(rows, -1),
-        value_a.reshape(rows, -1),
-        query_b.reshape(rows, -1),
-        key_b.reshape(rows, -1),
-        value_b.reshape(rows, -1),
-        par,
-    )
-    out_a = [got[at] for at, unit in enumerate(order) if unit[0] == "a"]
-    out_b = [got[at] for at, unit in enumerate(order) if unit[0] == "b"]
-    return jnp.concatenate(out_a, axis=1), functools.reduce(jnp.add, out_b)
-
-
 def zigzag_heads(query_a, key_a, value_a, query_b, key_b, value_b, mix_a, mix_b, gain_a, gain_b):
     head_gain_a, head_gain_b = gain_a, gain_b
     seq_rows = query_a.shape[0]
@@ -409,7 +199,13 @@
 
 
 def route_table(ids, weights, cap):
-    rows = ids.shape[0]
+    rows = ids.shape[1]
+    joined = [ids.astype(jnp.float32), weights, jnp.zeros((4, rows), jnp.float32)]
+    full = jnp.concatenate(joined, axis=0)
+    if rows < 128:
+        full = jnp.concatenate([full, jnp.zeros((8, 128 - rows), jnp.float32)], axis=1)
+    full = full.T[0:rows, :]
+    ids, weights = full[:, 0:2].astype(jnp.int32), full[:, 2:4]
     lane = lax.broadcasted_iota(jnp.int32, (rows, 128), 1)
     hits = [ids[:, which : which + 1] == lane for which in range(2)]
     named = jnp.where(hits[0], 1.0, 0.0) + jnp.where(hits[1], 1.0, 0.0)
@@ -430,22 +226,100 @@
     return table.T[0:8, :]
 
 
-def experts_kernel(
+def head_units(heads_a, heads_b):
+    half = heads_a // 2
+    order = [("a", head) for head in range(half)]
+    order += [("b", head) for head in range(heads_b)]
+    return order + [("a", head) for head in range(half, heads_a)]
+
+
+def chosen(me, units, for_a, for_b):
+    value = for_b(units[0][1]) if units[0][0] == "b" else for_a(units[0][1])
+    for at, (group, head) in enumerate(units):
+        if at:
+            value = jnp.where(me == at, for_a(head) if group == "a" else for_b(head), value)
+    return value
+
+
+def column(row):
+    return jnp.broadcast_to(row, (8, row.shape[1])).T[:, 0:1]
+
+
+def attend_block(chunk, block, queries, keys, values_t, heads, facts):
+    pick, scale, mix, gain, valid, share = facts
+    rows = queries.shape[1]
+    key = lax.broadcasted_iota(jnp.int32, (chunk, 2 * chunk), 0)
+    asks = lax.broadcasted_iota(jnp.int32, (chunk, 2 * chunk), 1)
+    allowed = key <= jnp.where(asks >= chunk, asks - chunk, asks)
+    for part in reversed(range(rows // chunk)):
+        first = part * chunk
+        before = block * rows + first
+        length = before + chunk
+        query = queries[block, first : first + chunk, :]
+        picked = jnp.concatenate([query * pick[0], query * pick[1]], axis=0)
+        scores = lax.dot_general(
+            keys[0:length, :],
+            picked,
+            (((1,), (1,)), ((), ())),
+            preferred_element_type=jnp.float32,
+        )
+        newest = jnp.where(allowed, scores[before:], NEG)
+        if before:
+            scores = jnp.concatenate([scores[:before], newest], axis=0)
+        else:
+            scores = newest
+        top = jnp.max(scores, axis=0, keepdims=True)
+        weights = jnp.exp2((scores - top) * scale)
+        sums = jnp.sum(weights, axis=0, keepdims=True)
+        found = jnp.dot(
+            values_t[:, 0:length], weights.astype(jnp.bfloat16), preferred_element_type=jnp.float32
+        )
+        found = found / sums
+        mixed = found[:, :chunk] - mix * found[:, chunk:]
+        square = jnp.sum(mixed * mixed * valid, axis=0, keepdims=True) * share
+        heads[block, :, first : first + chunk] = (
+            mixed * lax.rsqrt(square + EPS) * gain * HEAD_SCALE
+        ).astype(jnp.bfloat16)
+
+
+def layer_kernel(
     places,
     chips,
     cap,
-    term_ref,
+    units,
+    qa_ref,
+    ka_ref,
+    va_ref,
+    qb_ref,
+    kb_ref,
+    vb_ref,
+    mix_a_ref,
+    mix_b_ref,
+    gain_a_ref,
+    gain_b_ref,
     resid_ref,
     gain_ref,
     ids_ref,
     weights_ref,
+    proj_a_hbm,
+    proj_b_hbm,
     gate_hbm,
     up_hbm,
     down_hbm,
     out_ref,
+    ready_a,
+    ready_b,
+    got,
+    keys,
+    values_t,
+    heads,
+    joined,
+    turned,
+    proj,
     gate,
     up,
     down,
+    term,
     table,
     mixed,
     normed,
@@ -462,6 +336,10 @@
     back,
     leave,
     last,
+    ins,
+    inr,
+    outs,
+    outr,
     ws,
     ms,
     mr,
@@ -487,14 +365,135 @@
     other = 2 * chip + 1 - core
     rows, width = normed.shape
     slots = places * cap
-    loads = [
-        pltpu.make_async_copy(src, dst, ws.at[at])
-        for at, (src, dst) in enumerate(((gate_hbm, gate), (up_hbm, up), (down_hbm, down)))
-    ]
+    depth_a = proj_a_hbm.shape[0]
+    pairs = (
+        (proj_a_hbm, proj.at[0:depth_a]),
+        (proj_b_hbm, proj.at[depth_a : proj.shape[0]]),
+        (gate_hbm, gate),
+        (up_hbm, up),
+        (down_hbm, down),
+    )
+    loads = [pltpu.make_async_copy(src, dst, ws.at[at]) for at, (src, dst) in enumerate(pairs)]
     for load in loads:
         load.start()
+
+    seq, wide = qa_ref.shape[0], qa_ref.shape[2]
+    narrow = qb_ref.shape[2]
+    half = seq // 2
+    for at, ref in enumerate((qa_ref, ka_ref, va_ref)):
+        split = pltpu.einshape("abc->bac", ref[...])
+        for head in range(split.shape[0]):
+            ready_a[head, at * seq : (at + 1) * seq, :] = split[head]
+    asked, known, valued = [
+        pltpu.einshape("abc->bac", ref[...]) for ref in (qb_ref, kb_ref, vb_ref)
+    ]
+    for head in range(asked.shape[0]):
+        ready_b[head, 0:seq, :] = jnp.concatenate([asked[head], known[head]], axis=1)
+        ready_b[head, seq : seq + half, :] = jnp.concatenate(
+            [valued[head][:half], valued[head][half:]], axis=1
+        )
     table[0] = route_table(ids_ref[...], weights_ref[...], cap)
     greet_routes(places, chips)
+
+    sizes = [3 * seq if group == "a" else seq + half for group, _ in units]
+    spans, reach = [], {"a": 0, "b": depth_a}
+    for group, head in units:
+        tall = wide if group == "a" else narrow
+        spans.append((reach[group] + head * tall, tall))
+
+    def unit_ready(unit):
+        group, head = units[unit]
+        return (ready_a if group == "a" else ready_b).at[head]
+
+    def in_copy(unit, sender, away):
+        return remote(
+            unit_ready(unit),
+            got.at[sender, 0 : sizes[unit]],
+            ins.at[away],
+            inr.at[sender],
+            sp=unit,
+        )
+
+    def out_copy(unit, block):
+        start, tall = spans[unit]
+        return remote(
+            heads.at[block, 0:tall],
+            joined.at[start : start + tall],
+            outs.at[block],
+            outr.at[unit],
+            sp=block,
+        )
+
+    for away in reversed(range(1, places)):
+        for unit in range(places):
+
+            @pl.when(place == unit ^ away)
+            def _():
+                in_copy(unit, place, away).start()
+
+    def settle_block(sender, unit, held):
+        span = slice(sender * seq, (sender + 1) * seq)
+        if units[unit][0] == "a":
+            keys[span, :] = held[seq : 2 * seq, :]
+            values_t[:, span] = held[2 * seq : 3 * seq, :].T
+        else:
+            both = held[0:seq, :].astype(jnp.float32)
+            keys[span, :] = pltpu.roll(both, narrow, 1).astype(jnp.bfloat16)
+            packed = held[seq : seq + half, :].astype(jnp.float32).T
+            values_t[0:narrow, sender * seq : sender * seq + half] = packed[:narrow].astype(
+                jnp.bfloat16
+            )
+            values_t[0:narrow, sender * seq + half : (sender + 1) * seq] = packed[
+                narrow:
+            ].astype(jnp.bfloat16)
+            values_t[narrow:wide, span] = jnp.zeros((wide - narrow, seq), jnp.bfloat16)
+
+    for unit in range(places):
+
+        @pl.when(place == unit)
+        def _():
+            mine = unit_ready(unit)
+            got[unit, 0:seq] = mine[0:seq, :]
+            settle_block(unit, unit, mine)
+            for away in reversed(range(1, places)):
+                sender = unit ^ away
+                in_copy(unit, sender, away).wait_recv()
+                settle_block(sender, unit, got.at[sender])
+
+    is_a = chosen(place, units, lambda head: 1, lambda head: 0) == 1
+    lane = lax.broadcasted_iota(jnp.int32, (1, wide), 1)
+    map_wide = jnp.where(is_a, wide // 2, narrow // 2)
+    pick = []
+    for which in range(2):
+        inside = (lane >= which * map_wide) & (lane < (which + 1) * map_wide)
+        pick.append(jnp.where(inside, 1.0, 0.0).astype(jnp.bfloat16))
+    scale = jnp.where(
+        is_a,
+        math.log2(math.e) / math.sqrt(wide // 2),
+        math.log2(math.e) / math.sqrt(narrow // 2),
+    )
+    share = jnp.where(is_a, 1.0 / wide, 1.0 / narrow)
+    mix = chosen(place, units, lambda head: mix_a_ref[head], lambda head: mix_b_ref[head])
+    padded = jnp.concatenate(
+        [gain_b_ref[...], jnp.zeros((1, wide - narrow), jnp.float32)], axis=1
+    )
+    gain = column(jnp.where(is_a, gain_a_ref[...], padded))
+    valid = column(jnp.where(lane < jnp.where(is_a, wide, narrow), 1.0, 0.0))
+    facts = (pick, scale, mix, gain, valid, share)
+    chunk = math.gcd(seq, 256)
+    queries = got.at[:, 0:seq]
+    for block in reversed(range(places)):
+        attend_block(chunk, block, queries, keys, values_t, heads, facts)
+        for unit in range(places):
+
+            @pl.when(place == unit)
+            def _():
+                if unit == block:
+                    start, tall = spans[unit]
+                    joined[start : start + tall, :] = heads[block, 0:tall, :]
+                else:
+                    out_copy(unit, block).start()
+
     others = list(range(1, chips))
 
     def peer(apart):
@@ -506,7 +505,7 @@
         )
 
     def twin_copy(apart):
-        spot = term_ref.at[flipped(chip, apart), 1 - core]
+        spot = term.at[apart, 1 - core]
         return remote(spot, twin.at[apart], ts.at[apart], tr.at[apart], tp=other)
 
     def sum_copy(apart):
@@ -549,16 +548,28 @@
     def last_copy(apart):
         return remote(leave.at[apart], last.at[apart], ls.at[apart], lr.at[apart], tp=peer(apart))
 
+    for apart in others:
+        table_copy(apart).start()
+    for unit in range(places):
+
+        @pl.when(place != unit)
+        def _():
+            out_copy(unit, unit).wait_recv()
+
+    for load in loads[:2]:
+        load.wait()
+    turned[...] = joined[...].T
     turns = list(reversed(others)) + [0]
     for apart in turns:
+        first = pl.multiple_of(flipped(chip, apart) * (2 * rows), 2 * rows)
+        given = turned[pl.ds(first, 2 * rows), :]
+        summed = jnp.dot(given, proj[...], preferred_element_type=jnp.float32)
+        term[apart] = summed.astype(jnp.bfloat16).reshape(2, rows, width)
         twin_copy(apart).start()
-    for apart in others:
-        table_copy(apart).start()
     total = resid_ref[...].astype(jnp.float32)
     for apart in turns:
         twin_copy(apart).wait_recv()
-        both = term_ref[flipped(chip, apart), core].astype(jnp.float32)
-        both = both + twin[apart].astype(jnp.float32)
+        both = term[apart, core].astype(jnp.float32) + twin[apart].astype(jnp.float32)
         if apart:
             chip_sum[apart] = both.astype(jnp.bfloat16)
             sum_copy(apart).start()
@@ -652,7 +663,7 @@
     ahead = min(3, chips)
     for apart in range(ahead):
         send_out(apart)
-    for load in loads:
+    for load in loads[2:]:
         load.wait()
     for apart in range(chips):
         run_expert(apart)
@@ -670,6 +681,14 @@
         last_copy(apart).wait_recv()
         total = total + last[apart].astype(jnp.float32)
     out_ref[...] = total.astype(jnp.bfloat16)
+    for unit in range(places):
+
+        @pl.when(place == unit)
+        def _():
+            for away in range(1, places):
+                in_copy(unit ^ away, unit, away).wait_send()
+                out_copy(unit, unit ^ away).wait_send()
+
     for apart in range(chips):
         twin_copy(apart).wait_send()
         pair_copy(apart).wait_send()
@@ -688,27 +707,41 @@
     return [pl.BlockSpec(memory_space=pltpu.VMEM)] * count
 
 
-def routed_experts(
-    term, resid, norm_gain, route_ids, route_weights, capacity, gate, upward, down
-):
+def whole_layer(attention, resid, norm_gain, ids, weights, capacity, proj, experts):
+    query_a, key_a, value_a, query_b, key_b, value_b, mix_a, mix_b, gain_a, gain_b = attention
     places, chips = lax.axis_size("sp"), lax.axis_size("tp") // 2
     rows, width = resid.shape
-    deep = gate.shape[2]
+    seq, heads_a, wide = query_a.shape
+    heads_b, narrow = query_b.shape[1:]
+    deep = experts[0].shape[2]
     slots = places * capacity
+    tall = proj[0].shape[0] + proj[1].shape[0]
     sems = pltpu.SemaphoreType.DMA
+    units = head_units(heads_a, heads_b)
 
     def held(*shape):
         return pltpu.VMEM(shape, jnp.bfloat16)
 
+    smem = [pl.BlockSpec(memory_space=pltpu.SMEM)] * 2
     return pl.pallas_call(
-        functools.partial(experts_kernel, places, chips, capacity),
+        functools.partial(layer_kernel, places, chips, capacity, units),
         out_shape=jax.ShapeDtypeStruct((rows, width), jnp.bfloat16),
-        in_specs=vmem(5) + [pl.BlockSpec(memory_space=pl.ANY)] * 3,
+        in_specs=vmem(6) + smem + vmem(6) + [pl.BlockSpec(memory_space=pl.ANY)] * 5,
         out_specs=vmem(1)[0],
         scratch_shapes=[
+            held(heads_a, 3 * seq, wide),
+            held(heads_b, seq + seq // 2, wide),
+            held(places, 3 * seq, wide),
+            held(places * seq, wide),
+            held(wide, places * seq),
+            held(places, wide, seq),
+            held(tall, seq),
+            held(seq, tall),
+            held(tall, width),
             held(width, deep),
             held(width, deep),
             held(deep, width),
+            held(chips, 2, rows, width),
             pltpu.VMEM((chips, 8, 128), jnp.float32),
             pltpu.VMEM((rows, width), jnp.float32),
             held(rows, width),
@@ -725,7 +758,8 @@
             held(chips, places, capacity, width),
             held(chips, rows, width),
             held(chips, rows, width),
-            sems((3,)),
+            *[sems((places,))] * 4,
+            sems((5,)),
             *[sems((chips,))] * 8,
             *[sems((chips, places))] * 2,
             *[sems((chips,))] * 4,
@@ -733,17 +767,25 @@
             *[sems((chips,))] * 2,
         ],
         compiler_params=pltpu.CompilerParams(
-            collective_id=2, has_side_effects=True, vmem_limit_bytes=60 << 20
+            collective_id=1, has_side_effects=True, vmem_limit_bytes=67043328
         ),
     )(
-        term.reshape(chips, 2, rows, width),
+        query_a,
+        key_a,
+        value_a,
+        query_b,
+        key_b,
+        value_b,
+        mix_a,
+        mix_b,
+        gain_a[None, :],
+        gain_b[None, :],
         resid,
         norm_gain[None, :],
-        route_ids,
-        route_weights,
-        gate[0],
-        upward[0],
-        down[0],
+        ids.T,
+        weights.T,
+        *proj,
+        *[expert[0] for expert in experts],
     )
 
 
@@ -768,13 +810,12 @@
     expert_up,
     expert_down,
 ):
-    sp_ways = lax.axis_size("sp")
-    fits = query_a.shape[1] + query_b.shape[1] == sp_ways
-    whole_b = query_b.shape[1] * query_b.shape[2] == query_a.shape[2]
-    whole_b = whole_b and query_b.shape[2] == value_b.shape[2]
-    fits = fits and query_a.shape[2] == value_a.shape[2] and whole_b
-    attend = whole_heads if fits else zigzag_heads
-    heads_out_a, heads_out_b = attend(
+    sp_ways, tp_ways = lax.axis_size("sp"), lax.axis_size("tp")
+    width = resid.shape[1]
+    tok_rows = resid.shape[0]
+    top_count = route_ids.shape[1]
+    capacity = 3 * top_count * tok_rows // (2 * sp_ways)
+    attention = (
         query_a,
         key_a,
         value_a,
@@ -786,26 +827,25 @@
         head_gain_a,
         head_gain_b,
     )
-    width = resid.shape[1]
-    tok_rows = resid.shape[0]
-    top_count = route_ids.shape[1]
-    capacity = 3 * top_count * tok_rows // (2 * sp_ways)
-    term = jnp.dot(heads_out_a, proj_a, preferred_element_type=jnp.float32)
-    term = term + jnp.dot(heads_out_b, proj_b, preferred_element_type=jnp.float32)
-    tp_ways = lax.axis_size("tp")
+    wide, narrow = query_a.shape[2], query_b.shape[2]
+    fits = query_a.shape[1] + query_b.shape[1] == sp_ways and wide == 128 == 2 * narrow
+    fits = fits and wide == value_a.shape[2] and narrow == value_b.shape[2]
     paired = tp_ways % 2 == 0 and tp_ways & (tp_ways - 1) == 0 and sp_ways & (sp_ways - 1) == 0
-    if paired and top_count == 2 and capacity % 16 == 0 and tok_rows <= 128:
-        return routed_experts(
-            term.astype(jnp.bfloat16),
+    paired = paired and top_count == 2 and capacity % 16 == 0 and tok_rows <= 128
+    if fits and paired:
+        return whole_layer(
+            attention,
             resid,
             norm_gain,
             route_ids,
             route_weights,
             capacity,
-            expert_gate,
-            expert_up,
-            expert_down,
-        )
+            (proj_a, proj_b),
+            (expert_gate, expert_up, expert_down),
+        )
+    heads_out_a, heads_out_b = zigzag_heads(*attention)
+    term = jnp.dot(heads_out_a, proj_a, preferred_element_type=jnp.float32)
+    term = term + jnp.dot(heads_out_b, proj_b, preferred_element_type=jnp.float32)
     own_slots = slot_numbers(route_ids, sp_ways, capacity)
     mixed = resid.astype(jnp.float32) + lax.psum_scatter(
         lax.optimization_barrier(term.astype(jnp.bfloat16))

time: 177 us -> 155 us (0.88)
  Pallas kernels: 159 us -> 147 us
  local copies, waits for them, and re-layouts: 10.8 us -> 6.98 us
  other arithmetic: 3.53 us -> 0 us
  matrix products: 2.78 us -> 0 us
    pallas_call x2 -> x1, Pallas kernels: 159 us -> 147 us  [whole_layer(): pl.pallas_call(functools.partial(layer_kernel, places, chips, capacity, u...]
    reshape x4 -> x0, local copies, waits for them, and re-layouts: 4.18 us -> none  [the longest x1 1.1 us: whole_heads(): value_a.reshape(rows, -1)]
    dot_general x2 -> x0, matrix products: 2.78 us -> none  [the longest x1 2.06 us: per_device(): jnp.dot(heads_out_b, proj_b, preferred_element_type=jnp.float32)]
    unnamed x12 -> x4, local copies, waits for them, and re-layouts: 4.37 us -> 6.98 us
    another operation x1 -> x0, other arithmetic: 2.07 us -> none  [whole_heads(): jnp.stack([(mix_a if group == 'a' else mix_b)[head] for group, head in or...]
where the time goes in v2:
time: 155 us; the launch traced here: 154 us
  Pallas kernels  147 us (95%)
  local copies, waits for them, and re-layouts  6.98 us (5%)
    pallas_call x1, Pallas kernels, whole_layer(): pl.pallas_call(functools.partial(layer_kernel, places, chips, capacity, u...  147 us
    unnamed x4, local copies, waits for them, and re-layouts  6.98 us

profile of v2, /device:TPU:11, one launch (start us, length us, event | category | flops | bytes accessed | tf_op | source)
XLA Modules:
  0.0 154.4 jit_solution(12817734387738088108)
XLA Ops:
  0.0 1.8 %copy.20.qb_ref = bf16[512,2,64]{2,1,0:T(2,128)(2,1)} copy(bf16[512,2,64]{0,2,1:T(8,128)(2,1)} %param.23) | data formatting | bytes 262144 | tf_op args[4]
  1.8 1.8 %copy.21.kb_ref = bf16[512,2,64]{2,1,0:T(2,128)(2,1)} copy(bf16[512,2,64]{0,2,1:T(8,128)(2,1)} %param.24) | data formatting | bytes 262144 | tf_op args[5]
  3.5 1.8 %copy.22.vb_ref = bf16[512,2,64]{2,1,0:T(2,128)(2,1)} copy(bf16[512,2,64]{0,2,1:T(8,128)(2,1)} %param.25) | data formatting | bytes 262144 | tf_op args[6]
  5.3 147.4 %shard_map.181 = bf16[64,2048]{1,0:T(8,128)(2,1)} custom-call(bf16[512,2,128]{2,1,0:T(2,128)(2,1)} %qa_ref.1, bf16[512,2,128]{2,1,0:T(2,128)(2,1)} %ka_ref.1, bf16[512,2,128]{2,1,0:T(2,128)(2,1)} %va_ref.1, bf16[512,2,64]{2,1,0:T(2,128)(2,1)} %copy.20.qb_ref, bf16[512,2,64]{2,1,0:T(2,128)(2,1)} %copy.21.kb_ref, bf16[512,2,64]{2,1,0:T(2,128)(2,1)} %copy.22.vb_ref, ...), custom_call_target="tpu_custom_call" | custom-call | tf_op jit(solution)/shard_map/pallas_call | solution.py:726
  152.8 1.7 %copy.24 = bf16[64,2048]{1,0:T(8,128)(2,1)} copy(bf16[64,2048]{1,0:T(8,128)(2,1)} %shard_map.181) | data formatting | bytes 524288

commit v3 on v2

--- a/solution.py
+++ b/solution.py
@@ -307,9 +307,11 @@
     up_hbm,
     down_hbm,
     out_ref,
-    ready_a,
+    ready_q,
+    ready_k,
+    ready_v,
     ready_b,
-    got,
+    queries,
     keys,
     values_t,
     heads,
@@ -378,41 +380,46 @@
         load.start()
 
     seq, wide = qa_ref.shape[0], qa_ref.shape[2]
-    narrow = qb_ref.shape[2]
-    half = seq // 2
-    for at, ref in enumerate((qa_ref, ka_ref, va_ref)):
+    narrow = qb_ref.shape[1]
+    for ref, kept in ((qa_ref, ready_q), (ka_ref, ready_k)):
         split = pltpu.einshape("abc->bac", ref[...])
         for head in range(split.shape[0]):
-            ready_a[head, at * seq : (at + 1) * seq, :] = split[head]
-    asked, known, valued = [
-        pltpu.einshape("abc->bac", ref[...]) for ref in (qb_ref, kb_ref, vb_ref)
-    ]
-    for head in range(asked.shape[0]):
-        ready_b[head, 0:seq, :] = jnp.concatenate([asked[head], known[head]], axis=1)
-        ready_b[head, seq : seq + half, :] = jnp.concatenate(
-            [valued[head][:half], valued[head][half:]], axis=1
-        )
+            kept[head] = split[head]
+    split = pltpu.einshape("abc->bac", va_ref[...])
+    for head in range(split.shape[0]):
+        ready_v[head] = split[head].T
+    for head in range(qb_ref.shape[0]):
+        ready_b[head] = jnp.concatenate([qb_ref[head], kb_ref[head]], axis=0).T
     table[0] = route_table(ids_ref[...], weights_ref[...], cap)
     greet_routes(places, chips)
 
-    sizes = [3 * seq if group == "a" else seq + half for group, _ in units]
     spans, reach = [], {"a": 0, "b": depth_a}
     for group, head in units:
         tall = wide if group == "a" else narrow
         spans.append((reach[group] + head * tall, tall))
 
-    def unit_ready(unit):
+    def unit_parts(unit, sender):
         group, head = units[unit]
-        return (ready_a if group == "a" else ready_b).at[head]
-
-    def in_copy(unit, sender, away):
-        return remote(
-            unit_ready(unit),
-            got.at[sender, 0 : sizes[unit]],
-            ins.at[away],
-            inr.at[sender],
-            sp=unit,
-        )
+        first = sender * seq
+        if not isinstance(sender, int):
+            first = pl.multiple_of(first, seq)
+        span = pl.ds(first, seq)
+        if group == "a":
+            return (
+                (ready_q.at[head], queries.at[sender]),
+                (ready_k.at[head], keys.at[span, :]),
+                (ready_v.at[head], values_t.at[:, span]),
+            )
+        return (
+            (ready_b.at[head], queries.at[sender]),
+            (vb_ref.at[head], values_t.at[0:narrow, span]),
+        )
+
+    def in_copies(unit, sender, away):
+        return [
+            remote(src, dst, ins.at[away, at], inr.at[sender, at], sp=unit)
+            for at, (src, dst) in enumerate(unit_parts(unit, sender))
+        ]
 
     def out_copy(unit, block):
         start, tall = spans[unit]
@@ -429,36 +436,31 @@
 
             @pl.when(place == unit ^ away)
             def _():
-                in_copy(unit, place, away).start()
-
-    def settle_block(sender, unit, held):
-        span = slice(sender * seq, (sender + 1) * seq)
-        if units[unit][0] == "a":
-            keys[span, :] = held[seq : 2 * seq, :]
-            values_t[:, span] = held[2 * seq : 3 * seq, :].T
-        else:
-            both = held[0:seq, :].astype(jnp.float32)
-            keys[span, :] = pltpu.roll(both, narrow, 1).astype(jnp.bfloat16)
-            packed = held[seq : seq + half, :].astype(jnp.float32).T
-            values_t[0:narrow, sender * seq : sender * seq + half] = packed[:narrow].astype(
-                jnp.bfloat16
-            )
-            values_t[0:narrow, sender * seq + half : (sender + 1) * seq] = packed[
-                narrow:
-            ].astype(jnp.bfloat16)
-            values_t[narrow:wide, span] = jnp.zeros((wide - narrow, seq), jnp.bfloat16)
+                for copy in in_copies(unit, place, away):
+                    copy.start()
+
+    def swap_halves(sender):
+        both = queries[sender].astype(jnp.float32)
+        keys[sender * seq : (sender + 1) * seq, :] = pltpu.roll(both, narrow, 1).astype(
+            jnp.bfloat16
+        )
 
     for unit in range(places):
 
         @pl.when(place == unit)
         def _():
-            mine = unit_ready(unit)
-            got[unit, 0:seq] = mine[0:seq, :]
-            settle_block(unit, unit, mine)
+            packed = units[unit][0] == "b"
+            for src, dst in unit_parts(unit, unit):
+                dst[...] = src[...]
+            if packed:
+                values_t[narrow:wide, :] = jnp.zeros((wide - narrow, places * seq), jnp.bfloat16)
+                swap_halves(unit)
             for away in reversed(range(1, places)):
                 sender = unit ^ away
-                in_copy(unit, sender, away).wait_recv()
-                settle_block(sender, unit, got.at[sender])
+                for copy in in_copies(unit, sender, away):
+                    copy.wait_recv()
+                if packed:
+                    swap_halves(sender)
 
     is_a = chosen(place, units, lambda head: 1, lambda head: 0) == 1
     lane = lax.broadcasted_iota(jnp.int32, (1, wide), 1)
@@ -481,7 +483,6 @@
     valid = column(jnp.where(lane < jnp.where(is_a, wide, narrow), 1.0, 0.0))
     facts = (pick, scale, mix, gain, valid, share)
     chunk = math.gcd(seq, 256)
-    queries = got.at[:, 0:seq]
     for block in reversed(range(places)):
         attend_block(chunk, block, queries, keys, values_t, heads, facts)
         for unit in range(places):
@@ -613,33 +614,23 @@
         for away in range(1, places):
             route_copy(apart, away).wait_recv()
         pair_copy(apart).start()
+        if 0 < apart <= chips // 2:
+            settle(apart - 1)
         pair_copy(apart).wait_recv()
-        tile = 256
-
-        @pl.loop(0, hidden.shape[1] // tile)
-        def _(step):
-            cols = pl.ds(pl.multiple_of(step * tile, tile), tile)
-            given = piece[apart].reshape(2 * slots, width)
-            opened = jnp.dot(given, gate[:, cols], preferred_element_type=jnp.float32)
-            raised = jnp.dot(given, up[:, cols], preferred_element_type=jnp.float32)
-            hidden[:, cols] = (jax.nn.silu(opened) * raised).astype(jnp.bfloat16)
-
-        wide = 512
-
-        @pl.loop(0, width // wide)
-        def _(step):
-            cols = pl.ds(pl.multiple_of(step * wide, wide), wide)
-            lowered = jnp.dot(hidden[...], down[:, cols], preferred_element_type=jnp.float32)
-            part[apart, :, :, cols] = lowered.astype(jnp.bfloat16).reshape(2, slots, wide)
-
+        given = piece[apart].reshape(2 * slots, width)
+        opened = jnp.dot(given, gate[...], preferred_element_type=jnp.float32)
+        raised = jnp.dot(given, up[...], preferred_element_type=jnp.float32)
+        hidden[...] = (jax.nn.silu(opened) * raised).astype(jnp.bfloat16)
+        if apart + ahead < chips:
+            send_out(apart + ahead)
+        lowered = jnp.dot(hidden[...], down[...], preferred_element_type=jnp.float32)
+        part[apart] = lowered.astype(jnp.bfloat16).reshape(2, slots, width)
         part_copy(apart).start()
 
     def settle(apart):
         part_copy(apart).wait_recv()
         both = part[apart, core].astype(jnp.float32) + pair[apart].astype(jnp.float32)
         finished[apart] = both.astype(jnp.bfloat16).reshape(places, cap, width)
-        if apart:
-            send_back(apart)
 
     def send_back(apart):
         for away in reversed(range(1, places)):
@@ -667,13 +658,13 @@
         load.wait()
     for apart in range(chips):
         run_expert(apart)
-        if apart + ahead < chips:
-            send_out(apart + ahead)
-        if apart:
-            settle(apart - 1)
-    settle(chips - 1)
-    send_back(0)
-    for apart in others:
+        if apart >= chips // 2:
+            settle(apart)
+            send_back(apart)
+    nearer = list(range(1, chips // 2))
+    for apart in nearer + [0]:
+        send_back(apart)
+    for apart in list(range(chips // 2, chips)) + nearer:
         leave[apart] = gathered(apart).astype(jnp.bfloat16)
         last_copy(apart).start()
     total = mixed[...] + gathered(0)
@@ -686,7 +677,8 @@
         @pl.when(place == unit)
         def _():
             for away in range(1, places):
-                in_copy(unit ^ away, unit, away).wait_send()
+                for copy in in_copies(unit ^ away, unit, away):
+                    copy.wait_send()
                 out_copy(unit, unit ^ away).wait_send()
 
     for apart in range(chips):
@@ -729,9 +721,11 @@
         in_specs=vmem(6) + smem + vmem(6) + [pl.BlockSpec(memory_space=pl.ANY)] * 5,
         out_specs=vmem(1)[0],
         scratch_shapes=[
-            held(heads_a, 3 * seq, wide),
-            held(heads_b, seq + seq // 2, wide),
-            held(places, 3 * seq, wide),
+            held(heads_a, seq, wide),
+            held(heads_a, seq, wide),
+            held(heads_a, wide, seq),
+            held(heads_b, seq, wide),
+            held(places, seq, wide),
             held(places * seq, wide),
             held(wide, places * seq),
             held(places, wide, seq),
@@ -758,7 +752,8 @@
             held(chips, places, capacity, width),
             held(chips, rows, width),
             held(chips, rows, width),
-            *[sems((places,))] * 4,
+            *[sems((places, 3))] * 2,
+            *[sems((places,))] * 2,
             sems((5,)),
             *[sems((chips,))] * 8,
             *[sems((chips, places))] * 2,
@@ -773,9 +768,7 @@
         query_a,
         key_a,
         value_a,
-        query_b,
-        key_b,
-        value_b,
+        *[jnp.transpose(value, (1, 2, 0)) for value in (query_b, key_b, value_b)],
         mix_a,
         mix_b,
         gain_a[None, :],

time: 155 us -> 143 us (0.923)
  Pallas kernels: 147 us -> 141 us
  local copies, waits for them, and re-layouts: 6.98 us -> 1.67 us
    pallas_call x1, Pallas kernels: 147 us -> 141 us  [whole_layer(): pl.pallas_call(functools.partial(layer_kernel, places, chips, capacity, u...]
    unnamed x4 -> x1, local copies, waits for them, and re-layouts: 6.98 us -> 1.67 us
where the time goes in v3:
time: 143 us
  Pallas kernels  141 us (99%)
  local copies, waits for them, and re-layouts  1.67 us (1%)
    pallas_call x1, Pallas kernels, whole_layer(): pl.pallas_call(functools.partial(layer_kernel, places, chips, capacity, u...  141 us

profile of v3, /device:TPU:11, one launch (start us, length us, event | category | flops | bytes accessed | tf_op | source)
XLA Modules:
  0.0 142.7 jit_solution(17368995155157729436)
XLA Ops:
  0.0 141.0 %shard_map.181 = bf16[64,2048]{1,0:T(8,128)(2,1)} custom-call(bf16[512,2,128]{2,1,0:T(2,128)(2,1)} %qa_ref.1, bf16[512,2,128]{2,1,0:T(2,128)(2,1)} %ka_ref.1, bf16[512,2,128]{2,1,0:T(2,128)(2,1)} %va_ref.1, bf16[2,64,512]{2,1,0:T(8,128)(2,1)} %bitcast.14, bf16[2,64,512]{2,1,0:T(8,128)(2,1)} %bitcast.15, bf16[2,64,512]{2,1,0:T(8,128)(2,1)} %bitcast.16, ...), custom_call_target="tpu_custom_call" | custom-call | tf_op jit(solution)/shard_map/pallas_call | solution.py:718
  141.0 1.7 %copy.21 = bf16[64,2048]{1,0:T(8,128)(2,1)} copy(bf16[64,2048]{1,0:T(8,128)(2,1)} %shard_map.181) | data formatting | bytes 524288

commit v4 on v3

--- a/solution.py
+++ b/solution.py
@@ -186,7 +186,7 @@
         pl.semaphore_signal(
             barrier, inc=1, device_id=peer, device_id_type=pl.DeviceIdType.MESH
         )
-    pl.semaphore_wait(barrier, len(peers))
+    return functools.partial(pl.semaphore_wait, barrier, len(peers))
 
 
 def flipped(value, apart):
@@ -376,6 +376,7 @@
         (down_hbm, down),
     )
     loads = [pltpu.make_async_copy(src, dst, ws.at[at]) for at, (src, dst) in enumerate(pairs)]
+    all_here = greet_routes(places, chips)
     for load in loads:
         load.start()
 
@@ -391,7 +392,7 @@
     for head in range(qb_ref.shape[0]):
         ready_b[head] = jnp.concatenate([qb_ref[head], kb_ref[head]], axis=0).T
     table[0] = route_table(ids_ref[...], weights_ref[...], cap)
-    greet_routes(places, chips)
+    all_here()
 
     spans, reach = [], {"a": 0, "b": depth_a}
     for group, head in units:
@@ -509,10 +510,27 @@
         spot = term.at[apart, 1 - core]
         return remote(spot, twin.at[apart], ts.at[apart], tr.at[apart], tp=other)
 
-    def sum_copy(apart):
+    chunks = 2
+    chunk_rows = rows // chunks
+
+    def sum_copy(source, target, slot, to, lot):
+        span = slice(lot * chunk_rows, (lot + 1) * chunk_rows)
         return remote(
-            chip_sum.at[apart], sums.at[apart], rs.at[apart], rr.at[apart], tp=peer(apart)
-        )
+            chip_sum.at[source, span],
+            sums.at[target, span],
+            rs.at[source, lot],
+            rr.at[slot, lot],
+            tp=peer(to),
+        )
+
+    def beside_copy(lot):
+        return sum_copy(1, 1, 1, 1, lot)
+
+    def relay_copy(apart, lot):
+        return sum_copy(apart, apart ^ 1, apart ^ 1, 1, lot)
+
+    def across_copy(apart, lot):
+        return sum_copy(apart, 0, 0, apart, lot)
 
     def near_copy(apart):
         return remote(normed, near.at[apart], zs.at[apart], zr.at[apart], tp=peer(apart))
@@ -561,6 +579,7 @@
         load.wait()
     turned[...] = joined[...].T
     turns = list(reversed(others)) + [0]
+    outer = (chip == 0) | (chip == chips - 1)
     for apart in turns:
         first = pl.multiple_of(flipped(chip, apart) * (2 * rows), 2 * rows)
         given = turned[pl.ds(first, 2 * rows), :]
@@ -573,12 +592,31 @@
         both = term[apart, core].astype(jnp.float32) + twin[apart].astype(jnp.float32)
         if apart:
             chip_sum[apart] = both.astype(jnp.bfloat16)
-            sum_copy(apart).start()
+            for lot in range(chunks):
+                if apart == 1:
+                    beside_copy(lot).start()
+                else:
+                    pl.when(outer)(relay_copy(apart, lot).start)
         else:
             total = total + both
-    for apart in others:
-        sum_copy(apart).wait_recv()
-        total = total + sums[apart].astype(jnp.float32)
+
+    @pl.when(jnp.logical_not(outer))
+    def _():
+        for apart in (2, 3):
+            for lot in range(chunks):
+                span = slice(lot * chunk_rows, (lot + 1) * chunk_rows)
+                relay_copy(apart ^ 1, lot).wait_recv()
+                both = chip_sum[apart, span, :].astype(jnp.float32)
+                both = both + sums[apart, span, :].astype(jnp.float32)
+                chip_sum[apart, span, :] = both.astype(jnp.bfloat16)
+                across_copy(apart, lot).start()
+
+    for lot in range(chunks):
+        beside_copy(lot).wait_recv()
+    total = total + sums[1].astype(jnp.float32)
+    for lot in range(chunks):
+        across_copy(2, lot).wait_recv()
+    total = total + sums[0].astype(jnp.float32)
     mixed[...] = total
     normed[...] = rms_scaled(total, gain_ref[...]).astype(jnp.bfloat16)
     for apart in others:
@@ -687,7 +725,8 @@
         part_copy(apart).wait_send()
         if apart:
             table_copy(apart).wait_send()
-            sum_copy(apart).wait_send()
+            for lot in range(chunks):
+                across_copy(apart, lot).wait_send()
             near_copy(apart).wait_send()
             last_copy(apart).wait_send()
         for away in range(1, places):
@@ -755,7 +794,9 @@
             *[sems((places, 3))] * 2,
             *[sems((places,))] * 2,
             sems((5,)),
-            *[sems((chips,))] * 8,
+            *[sems((chips,))] * 4,
+            *[sems((chips, 2))] * 2,
+            *[sems((chips,))] * 2,
             *[sems((chips, places))] * 2,
             *[sems((chips,))] * 4,
             *[sems((chips, places))] * 2,
@@ -825,7 +866,7 @@
     fits = fits and wide == value_a.shape[2] and narrow == value_b.shape[2]
     paired = tp_ways % 2 == 0 and tp_ways & (tp_ways - 1) == 0 and sp_ways & (sp_ways - 1) == 0
     paired = paired and top_count == 2 and capacity % 16 == 0 and tok_rows <= 128
-    if fits and paired:
+    if fits and paired and tp_ways == 8:
         return whole_layer(
             attention,
             resid,

time: 143 us -> 141 us (0.986); the launches traced: 143 us -> 138 us
  Pallas kernels: 141 us -> 137 us
    pallas_call x1, Pallas kernels: 141 us -> 137 us  [whole_layer(): pl.pallas_call(functools.partial(layer_kernel, places, chips, capacity, u...]
where the time goes in v4:
time: 141 us; the launch traced here: 138 us
  Pallas kernels  137 us (97%)
  local copies, waits for them, and re-layouts  1.67 us (1%)
    pallas_call x1, Pallas kernels, whole_layer(): pl.pallas_call(functools.partial(layer_kernel, places, chips, capacity, u...  137 us

profile of v4, /device:TPU:11, one launch (start us, length us, event | category | flops | bytes accessed | tf_op | source)
XLA Modules:
  0.0 138.4 jit_solution(8734574746827665457)
XLA Ops:
  0.0 136.7 %shard_map.181 = bf16[64,2048]{1,0:T(8,128)(2,1)} custom-call(bf16[512,2,128]{2,1,0:T(2,128)(2,1)} %qa_ref.1, bf16[512,2,128]{2,1,0:T(2,128)(2,1)} %ka_ref.1, bf16[512,2,128]{2,1,0:T(2,128)(2,1)} %va_ref.1, bf16[2,64,512]{2,1,0:T(8,128)(2,1)} %bitcast.14, bf16[2,64,512]{2,1,0:T(8,128)(2,1)} %bitcast.15, bf16[2,64,512]{2,1,0:T(8,128)(2,1)} %bitcast.16, ...), custom_call_target="tpu_custom_call" | custom-call | tf_op jit(solution)/shard_map/pallas_call | solution.py:757
  136.8 1.7 %copy.21 = bf16[64,2048]{1,0:T(8,128)(2,1)} copy(bf16[64,2048]{1,0:T(8,128)(2,1)} %shard_map.181) | data formatting | bytes 524288
